TPU v7x, 512 devices: a whole 4x4x16 slice. The times are simulated.
512 devices in a mesh: sp: 16 (over y, x), tp: 32 (over z, core).
Axes of the slice: x: 4, y: 4, z: 16, core: 2. Of those that a mesh axis runs over, the one named last changes fastest.
Arguments:
- target: bfloat16 [2048, 2048], P('sp'), may hold values from -6 to 6
- source: bfloat16 [6144, 2048], P('sp'), may hold values from -6 to 6
- cotangent: bfloat16 [2048, 2048], P('sp'), may hold values from -192 to 192
- target_gain: float32 [2048], replicated, may hold values from 0.1 to 1.9
- source_gain: float32 [2048], replicated, may hold values from 0.1 to 1.9
- w_query: bfloat16 [2048, 4096], P(None, 'tp'), may hold values from -0.125 to 0.125
- w_key: bfloat16 [2048, 128], replicated, may hold values from -0.125 to 0.125
- w_value: bfloat16 [2048, 128], replicated, may hold values from -0.125 to 0.125
- w_out: bfloat16 [4096, 2048], P('tp'), may hold values from -0.09375 to 0.09375
Outputs:
- grad_target: bfloat16 [2048, 2048], P(('sp', 'tp'))
- grad_source: bfloat16 [6144, 2048], P(('sp', 'tp'))
- grad_out_w: bfloat16 [4096, 2048], P('tp', 'sp')
All inputs are finite; a program needn't handle non-finite values.
Results may differ from a plain program's by a relative error of at most 0.025.
Values may be sent and summed in bfloat16 or wider, within the bound.
A program may use at most 64 MiB of HBM per device.

v0:
```python
import jax
import jax.numpy as jnp
from jax import lax
from jax.sharding import Mesh
from jax.sharding import PartitionSpec as P

HEAD = 128
SP = ("sp_0", "sp_1")
SP_TP = ("sp_0", "sp_1", "tp")


NORM_EPS = 1e-06
KEY_BLOCK = 1024
QUERY_BLOCK = 256


def in_one_piece(arrays, axis, dim, along):
    ends, at = ([], 0)
    for a in arrays[:-1]:
        at += a.shape[along]
        ends.append(at)
    both = jnp.concatenate(arrays, axis=along)
    return tuple(jnp.split(lax.all_gather(both, axis, axis=dim, tiled=True), ends, axis=along))


def in_blocks(x, dim, count):
    before, after = (x.shape[:dim], x.shape[dim + 1 :])
    return jnp.moveaxis(x.reshape(*before, count, -1, *after), dim, 0)


def sum_at_owner(x, axis, dim):
    blocks = in_blocks(x, dim, lax.axis_size(axis))
    arrived = lax.all_to_all(blocks, axis, split_axis=0, concat_axis=0, tiled=True)
    return arrived.astype(jnp.float32).sum(axis=0)


def sent_together(arrays, axis, dim, along):
    widths = [a.shape[along] for a in arrays]
    both = jnp.concatenate(arrays, axis=along)
    result = sum_at_owner(both, axis, dim)
    return tuple(jnp.split(result, [sum(widths[:k]) for k in range(1, len(widths))], axis=along))


def whole_of(x, axes, dim):
    result = x
    for number in range(len(axes) - 1, -1, -1):
        result = lax.all_gather(result, axes[number], axis=dim, tiled=True)
    return result


def normed(row_block, gain_vec):
    rows_wide = row_block.astype(jnp.float32)
    inv_rms = lax.rsqrt(jnp.mean(rows_wide * rows_wide, axis=1, keepdims=True) + NORM_EPS)
    return (rows_wide * inv_rms * gain_vec).astype(jnp.bfloat16)


def norm_back(row_block, gain_vec, upstream):
    rows_wide = row_block.astype(jnp.float32)
    inv_rms = lax.rsqrt(jnp.mean(rows_wide * rows_wide, axis=1, keepdims=True) + NORM_EPS)
    unit_rows = rows_wide * inv_rms
    pulled = upstream * gain_vec
    return inv_rms * (pulled - unit_rows * jnp.mean(pulled * unit_rows, axis=1, keepdims=True))


def right_product(left_rows, weight_mat):
    return lax.dot_general(
        left_rows, weight_mat, (((1,), (1,)), ((), ())), preferred_element_type=jnp.float32
    )


def on_device(target, source, cotangent, target_gain, source_gain, w_query, w_key, w_value, w_out):
    tp_count = lax.axis_size("tp")
    tp_place = lax.axis_index("tp")
    group_rows = target.shape[0]
    q_width = w_query.shape[1]
    heads_here = q_width // HEAD
    inv_root = HEAD ** (-0.5)
    query_all = jnp.dot(
        normed(target, target_gain), w_query, preferred_element_type=jnp.float32
    ).astype(jnp.bfloat16)
    grad_all = right_product(cotangent, w_out).astype(jnp.bfloat16)
    cot_columns = lax.all_to_all(cotangent, SP, split_axis=1, concat_axis=0, tiled=True)
    source_rows = source.shape[0] // tp_count
    source_part = lax.dynamic_slice_in_dim(source, tp_place * source_rows, source_rows, 0)
    source_normed = normed(source_part, source_gain)
    key_own = jnp.dot(source_normed, w_key, preferred_element_type=jnp.float32).astype(jnp.bfloat16)
    value_own = jnp.dot(source_normed, w_value, preferred_element_type=jnp.float32).astype(
        jnp.bfloat16
    )
    key_group, value_group = in_one_piece((key_own, value_own), "tp", 0, 1)
    query_heads = query_all.reshape(group_rows, heads_here, HEAD)
    grad_heads = grad_all.reshape(group_rows, heads_here, HEAD)
    empty_stat = jnp.zeros((group_rows, heads_here), jnp.float32)
    empty_acc = jnp.zeros((group_rows, heads_here, HEAD), jnp.float32)
    start_state = (empty_stat, empty_acc, empty_acc, empty_acc)
    key_every, value_every = in_one_piece((key_group, value_group), SP, 0, 1)
    piece_rows = key_every.shape[0]
    step_rows = KEY_BLOCK

    def attend_one_block(block_index, loop_state):
        row_total, output_sum, tilted_sum, weight_sum = loop_state
        key_block = lax.dynamic_slice_in_dim(key_every, block_index * step_rows, step_rows, 0)
        value_block = lax.dynamic_slice_in_dim(value_every, block_index * step_rows, step_rows, 0)
        scores = (
            jnp.einsum("ihd,jd->ihj", query_heads, key_block, preferred_element_type=jnp.float32)
            * inv_root
        )
        exponent = jnp.exp(scores)
        weights = exponent.astype(jnp.bfloat16)
        prob_grad = jnp.einsum(
            "ihd,jd->ihj", grad_heads, value_block, preferred_element_type=jnp.float32
        )
        tilted = (exponent * prob_grad).astype(jnp.bfloat16)
        row_total = row_total + jnp.sum(exponent, axis=2)
        output_sum = output_sum + jnp.einsum(
            "ihj,jd->ihd", weights, value_block, preferred_element_type=jnp.float32
        )
        tilted_sum = tilted_sum + jnp.einsum(
            "ihj,jd->ihd", tilted, key_block, preferred_element_type=jnp.float32
        )
        weight_sum = weight_sum + jnp.einsum(
            "ihj,jd->ihd", weights, key_block, preferred_element_type=jnp.float32
        )
        return (row_total, output_sum, tilted_sum, weight_sum)

    row_total, output_sum, tilted_sum, weight_sum = lax.fori_loop(
        0, piece_rows // step_rows, attend_one_block, start_state
    )
    attended = (output_sum / row_total[:, :, None]).astype(jnp.bfloat16)
    delta_row = jnp.sum(attended.astype(jnp.float32) * grad_heads.astype(jnp.float32), axis=2)
    grad_query = (
        (tilted_sum - delta_row[:, :, None] * weight_sum) / row_total[:, :, None] * inv_root
    ).astype(jnp.bfloat16)
    all_total, all_delta = in_one_piece((row_total, delta_row), SP, 0, 1)
    empty_keys = jnp.zeros((key_group.shape[0], HEAD), jnp.float32)
    query_piece, grad_piece = in_one_piece((query_all, grad_all), SP, 0, 1)
    piece_rows = query_piece.shape[0]
    collect_step_rows = QUERY_BLOCK

    def collect_one_block(block_index, loop_state):
        key_grad, value_grad = loop_state
        local_begin = block_index * collect_step_rows
        query_block = lax.dynamic_slice_in_dim(
            query_piece, local_begin, collect_step_rows, 0
        ).reshape(collect_step_rows, heads_here, HEAD)
        grad_block = lax.dynamic_slice_in_dim(
            grad_piece, local_begin, collect_step_rows, 0
        ).reshape(collect_step_rows, heads_here, HEAD)
        total_block = lax.dynamic_slice_in_dim(all_total, local_begin, collect_step_rows, 0)
        delta_block = lax.dynamic_slice_in_dim(all_delta, local_begin, collect_step_rows, 0)
        scores = (
            jnp.einsum("ihd,jd->ihj", query_block, key_group, preferred_element_type=jnp.float32)
            * inv_root
        )
        prob_rows = jnp.exp(scores) / total_block[:, :, None]
        prob_grad = jnp.einsum(
            "ihd,jd->ihj", grad_block, value_group, preferred_element_type=jnp.float32
        )
        score_grad = (prob_rows * (prob_grad - delta_block[:, :, None])).astype(jnp.bfloat16)
        key_grad = (
            key_grad
            + jnp.einsum("ihj,ihd->jd", score_grad, query_block, preferred_element_type=jnp.float32)
            * inv_root
        )
        value_grad = value_grad + jnp.einsum(
            "ihj,ihd->jd",
            prob_rows.astype(jnp.bfloat16),
            grad_block,
            preferred_element_type=jnp.float32,
        )
        return (key_grad, value_grad)

    key_grad, value_grad = lax.fori_loop(
        0, piece_rows // collect_step_rows, collect_one_block, (empty_keys, empty_keys)
    )
    key_sum, value_sum = sent_together(
        (key_grad.astype(jnp.bfloat16), value_grad.astype(jnp.bfloat16)), "tp", 0, 1
    )
    pulled_source = right_product(key_sum.astype(jnp.bfloat16), w_key) + right_product(
        value_sum.astype(jnp.bfloat16), w_value
    )
    grad_source = norm_back(source_part, source_gain, pulled_source).astype(jnp.bfloat16)
    query_grad_rows = grad_query.reshape(group_rows, q_width)
    target_rows = group_rows // tp_count
    pulled_target = sum_at_owner(
        right_product(query_grad_rows, w_query).astype(jnp.bfloat16), "tp", 0
    )
    target_part = lax.dynamic_slice_in_dim(target, tp_place * target_rows, target_rows, 0)
    grad_target = norm_back(target_part, target_gain, pulled_target).astype(jnp.bfloat16)
    attended_rows = attended.reshape(group_rows, q_width)
    grad_out = lax.dot_general(
        whole_of(attended_rows, SP, 0),
        cot_columns,
        (((0,), (0,)), ((), ())),
        preferred_element_type=jnp.float32,
    )
    return (grad_target, grad_source, grad_out.astype(jnp.bfloat16))


def solution(mesh):
    split = Mesh(mesh.devices.reshape(4, 4, mesh.shape["tp"]), ("sp_0", "sp_1", "tp"))
    in_specs = (
        P(SP, None),
        P(SP, None),
        P(SP, None),
        P(),
        P(),
        P(None, "tp"),
        P(),
        P(),
        P("tp", None),
    )
    out_specs = (P(SP_TP, None), P(SP_TP, None), P("tp", SP))
    return jax.shard_map(
        on_device, mesh=split, in_specs=in_specs, out_specs=out_specs, check_vma=False
    )
```

profile of v0, /device:TPU:1, one launch (start us, length us, event | category | flops | bytes accessed | tf_op | source)
XLA Modules:
  0.0 299.7 jit_solution(13140715405996639786)
XLA Ops:
  7.3 1.3 fusion.43
  8.6 1.6 convolution_convert_fusion.2
  11.3 1.0 fusion.58
  12.4 1.1 convolution_convert_fusion.4
  13.6 1.1 convolution_convert_fusion.5
  14.7 38.3 %all-gather.2 = bf16[32,12,256]{2,1,0:T(8,128)(2,1)S(1)} all-gather(bf16[1,12,256]{2,1,0:T(8,128)(2,1)S(1)} %maximum_bitcast_fusion), channel_id=1, replica_groups=mesh['sp_0'=4,'sp_1'=4,'tp'=32] {'tp'}, dimensions={0}, use_global_device_ids=true | all-gather | bytes 202752 | tf_op jit(solution)/shard_map/all_gather | solution.py:23
  53.7 1.0 copy.42
  54.8 6.8 %all-to-all-start.2 = ((bf16[128,16,128]{0,2,1:T(8,128)(2,1)}), bf16[128,16,128]{0,2,1:T(8,128)(2,1)}, u32[]{:S(2)}, u32[]{:S(2)}) async-start(bf16[128,16,128]{0,2,1:T(8,128)(2,1)} %bitcast.7), calls=%async_computation.2 | async-start | bytes 1048576 | tf_op jit(solution)/shard_map/all_to_all | solution.py:82
  61.9 15.8 %all-gather.8.cloned.1.call-done = bf16[2048,256]{0,1:T(8,128)(2,1)} async-done(((bf16[128,256]{0,1:T(8,128)(2,1)}), bf16[2048,256]{0,1:T(8,128)(2,1)}) %all-gather.8.cloned.1.call-update) | async-done | bytes 1048592 | tf_op jit(solution)/shard_map/all_gather | solution.py:23
  77.7 2.3 fusion.79
  80.0 61.0 %all-gather.6.cloned.1.call-done = bf16[6144,256]{1,0:T(8,128)(2,1)} async-done(((bf16[384,256]{1,0:T(8,128)(2,1)}), bf16[6144,256]{1,0:T(8,128)(2,1)}) %all-gather.6.cloned.1.call-update) | async-done | bytes 3145744 | tf_op jit(solution)/shard_map/all_gather | solution.py:23
  141.0 3.2 %fusion.78 = (bf16[6144,128]{1,0:T(8,128)(2,1)}, bf16[6144,128]{1,0:T(8,128)(2,1)S(1)}) fusion(bf16[6144,256]{1,0:T(8,128)(2,1)} %all-gather.6.cloned.1.call-done), kind=kLoop, calls=%fused_computation.106 | loop fusion | bytes 6291456 | tf_op jit(solution)/shard_map/split | solution.py:23
  144.2 20.0 %while.36 = (s32[]{:T(128)}, f32[128,1]{0,1:T(1,128)S(1)}, f32[128,1,128]{2,0,1:T(8,128)S(1)}, f32[128,1,128]{2,0,1:T(8,128)S(1)}, f32[128,1,128]{2,0,1:T(8,128)...) while((s32[]{:T(128)}, f32[128,1]{0,1:T(1,128)S(1)}, ...), condition=%wide.region_5.0_spmd.clone, body=%wide.region_3.5_spmd.clone.sunk | while | flops 168657024 | bytes 3870403 | solution.py:126
  144.5 1.4 fusion.124
  146.3 1.2 fusion.123
  147.9 1.4 fusion.124
  149.6 1.2 fusion.123
  151.2 1.4 fusion.124
  153.0 1.2 fusion.123
  154.5 1.4 fusion.124
  156.3 1.2 fusion.123
  157.9 1.4 fusion.124
  159.6 1.2 fusion.123
  161.2 1.4 fusion.124
  163.0 1.2 fusion.123
  164.4 16.8 %all_gather.21 = f32[2048,2]{0,1:T(2,128)S(1)} all-gather(f32[128,2]{0,1:T(2,128)S(1)} %pad_maximum_fusion.2), channel_id=1, replica_groups=mesh['sp_0'=4,'sp_1'=4,'tp'=32] {'sp_0','sp_1'}, dimensions={0}, use_global_device_ids=true | all-gather | bytes 17408 | tf_op jit(solution)/shard_map/all_gather | solution.py:23
  181.2 29.4 %while.37 = (s32[]{:T(128)}, f32[384,128]{1,0:T(8,128)S(1)}, f32[384,128]{1,0:T(8,128)S(1)}, bf16[2048,128]{0,1:T(8,128)(2,1)}, bf16[384,128]{1,0:T(8,128)(2,1)S...) while((s32[]{:T(128)}, f32[384,128]{1,0:T(8,128)S(1)}, ...), condition=%wide.region_10.0_spmd.clone, body=%wide.region_9.0_spmd.clone.sunk | while | flops 101498880 | bytes 2432705 | solution.py:173
  181.2 1.1 fusion.133
  182.3 1.1 convolution_add_fusion.3
  183.5 1.4 fusion.134
  184.9 1.1 fusion.133
  186.0 1.1 convolution_add_fusion.3
  187.1 1.4 fusion.134
  188.6 1.1 fusion.133
  189.7 1.1 convolution_add_fusion.3
  190.8 1.4 fusion.134
  192.2 1.1 fusion.133
  193.3 1.1 convolution_add_fusion.3
  194.5 1.4 fusion.134
  195.9 1.1 fusion.133
  197.0 1.1 convolution_add_fusion.3
  198.1 1.4 fusion.134
  199.6 1.1 fusion.133
  200.7 1.1 convolution_add_fusion.3
  201.8 1.4 fusion.134
  203.3 1.1 fusion.133
  204.4 1.1 convolution_add_fusion.3
  205.5 1.4 fusion.134
  206.9 1.1 fusion.133
  208.0 1.1 convolution_add_fusion.3
  209.2 1.4 fusion.134
  211.4 18.9 %all-to-all-start.1 = ((bf16[32,12,256]{2,1,0:T(8,128)(2,1)}), bf16[32,12,256]{2,1,0:T(8,128)(2,1)S(1)}, u32[]{:S(2)}, u32[]{:S(2)}) async-start(bf16[32,12,256]{2,1,0:T(8,128)(2,1)} %reshape.147), calls=%async_computation.1 | async-start | bytes 524288 | tf_op jit(solution)/shard_map/all_to_all | solution.py:33
  230.8 1.0 reshape.146
  231.8 20.7 %all-to-all-done.1 = bf16[32,12,256]{2,1,0:T(8,128)(2,1)S(1)} async-done(((bf16[32,12,256]{2,1,0:T(8,128)(2,1)}), bf16[32,12,256]{2,1,0:T(8,128)(2,1)S(1)}, u32[]{:S(2)}, u32[]{:S(2)}) %all-to-all-start.1) | async-done | bytes 196640 | tf_op jit(solution)/shard_map/all_to_all | solution.py:33
  252.5 4.2 %all-to-all-start = ((bf16[32,4,2048]{2,1,0:T(4,128)(2,1)}), bf16[32,4,2048]{2,1,0:T(4,128)(2,1)S(1)}, u32[]{:S(2)}, u32[]{:S(2)}) async-start(bf16[32,4,2048]{2,1,0:T(4,128)(2,1)} %reshape.146), calls=%async_computation | async-start | bytes 1048576 | tf_op jit(solution)/shard_map/all_to_all | solution.py:33
  257.7 1.4 copy.43
  259.0 9.4 %all-gather = bf16[512,1,128]{0,2,1:T(8,128)(2,1)S(1)} all-gather(bf16[128,1,128]{0,2,1:T(8,128)(2,1)S(1)} %get-tuple-element.490), channel_id=2, replica_groups=mesh['sp_0'=4,'sp_1'=4,'tp'=32] {'sp_1'}, dimensions={0}, use_global_device_ids=true | all-gather | bytes 163840 | tf_op jit(solution)/shard_map/all_gather | solution.py:47
  268.4 11.4 %all-gather.1 = bf16[2048,1,128]{0,2,1:T(8,128)(2,1)S(1)} all-gather(bf16[512,1,128]{0,2,1:T(8,128)(2,1)S(1)} %all-gather), channel_id=3, replica_groups=mesh['sp_0'=4,'sp_1'=4,'tp'=32] {'sp_0'}, dimensions={0}, use_global_device_ids=true | all-gather | bytes 655360 | tf_op jit(solution)/shard_map/all_gather | solution.py:47
  279.9 0.9 convolution_convert_fusion.1
  281.1 1.3 fusion.54
  282.4 1.6 fusion.57
  284.0 6.3 %all-to-all-done = bf16[32,4,2048]{2,1,0:T(4,128)(2,1)S(1)} async-done(((bf16[32,4,2048]{2,1,0:T(4,128)(2,1)}), bf16[32,4,2048]{2,1,0:T(4,128)(2,1)S(1)}, u32[]{:S(2)}, u32[]{:S(2)}) %all-to-all-start) | async-done | bytes 524320 | tf_op jit(solution)/shard_map/all_to_all | solution.py:33
  290.5 1.0 fusion.61
  291.5 1.4 fusion.64
  (84 shorter events, 8.8 us)
Async XLA Ops:
  7.2 3.0 %copy-start = (bf16[2048,128]{1,0:T(8,128)(2,1)S(1)}, bf16[2048,128]{1,0:T(8,128)(2,1)}, u32[]{:S(2)}) copy-start(bf16[2048,128]{1,0:T(8,128)(2,1)} %param.18) | copy-start | bytes 1572868
  7.2 3.0 %copy-start.7 = (bf16[128,2048]{1,0:T(8,128)(2,1)S(1)}, bf16[128,2048]{1,0:T(8,128)(2,1)}, u32[]{:S(2)}) copy-start(bf16[128,2048]{1,0:T(8,128)(2,1)} %param.13) | copy-start | bytes 1572868
  7.2 3.0 %copy-start.9 = (f32[2048]{0:T(1024)S(1)}, f32[2048]{0:T(1024)}, u32[]{:S(2)}) copy-start(f32[2048]{0:T(1024)} %param.16) | copy-start | bytes 24580
  7.2 5.2 %copy-start.8 = (f32[2048]{0:T(1024)S(1)}, f32[2048]{0:T(1024)}, u32[]{:S(2)}) copy-start(f32[2048]{0:T(1024)} %param.17) | copy-start | bytes 24580
  7.2 5.2 %copy-start.3 = (bf16[2048,128]{1,0:T(8,128)(2,1)S(1)}, bf16[2048,128]{1,0:T(8,128)(2,1)}, u32[]{:S(2)}) copy-start(bf16[2048,128]{1,0:T(8,128)(2,1)} %param.20) | copy-start | bytes 1572868
  7.2 70.5 %all-gather.8.cloned.1.call-start = ((), (), s32[]{:S(2)}) async-start(), calls=%async_computation.4 | async-start | bytes 1114112 | tf_op jit(solution)/shard_map/all_gather | solution.py:23
  8.6 4.9 %copy-start.1 = (bf16[2048,128]{1,0:T(8,128)(2,1)S(1)}, bf16[2048,128]{1,0:T(8,128)(2,1)}, u32[]{:S(2)}) copy-start(bf16[2048,128]{1,0:T(8,128)(2,1)} %param.19) | copy-start | bytes 1572868
  10.2 43.5 %copy-start.5 = (bf16[128,2048]{1,0:T(8,128)(2,1)S(1)}, bf16[128,2048]{1,0:T(8,128)(2,1)}, u32[]{:S(2)}) copy-start(bf16[128,2048]{1,0:T(8,128)(2,1)} %param.15) | copy-start | bytes 1572868
  11.3 129.7 %all-gather.6.cloned.1.call-start = ((), (), s32[]{:S(2)}) async-start(), calls=%async_computation.3 | async-start | bytes 3342336 | tf_op jit(solution)/shard_map/all_gather | solution.py:23
  53.7 8.2 %copy-start.6 = (bf16[384,256]{1,0:T(8,128)(2,1)S(1)}, bf16[384,256]{1,0:T(8,128)(2,1)}, u32[]{:S(2)}) copy-start(bf16[384,256]{1,0:T(8,128)(2,1)} %reshape.152) | copy-start | bytes 589828
  54.8 156.6 %all-to-all-start.2 = ((bf16[128,16,128]{0,2,1:T(8,128)(2,1)}), bf16[128,16,128]{0,2,1:T(8,128)(2,1)}, u32[]{:S(2)}, u32[]{:S(2)}) async-start(bf16[128,16,128]{0,2,1:T(8,128)(2,1)} %bitcast.7), calls=%async_computation.2 | async-start | bytes 1048576 | tf_op jit(solution)/shard_map/all_to_all | solution.py:82
  211.4 41.2 %all-to-all-start.1 = ((bf16[32,12,256]{2,1,0:T(8,128)(2,1)}), bf16[32,12,256]{2,1,0:T(8,128)(2,1)S(1)}, u32[]{:S(2)}, u32[]{:S(2)}) async-start(bf16[32,12,256]{2,1,0:T(8,128)(2,1)} %reshape.147), calls=%async_computation.1 | async-start | bytes 524288 | tf_op jit(solution)/shard_map/all_to_all | solution.py:33
  252.5 37.7 %all-to-all-start = ((bf16[32,4,2048]{2,1,0:T(4,128)(2,1)}), bf16[32,4,2048]{2,1,0:T(4,128)(2,1)S(1)}, u32[]{:S(2)}, u32[]{:S(2)}) async-start(bf16[32,4,2048]{2,1,0:T(4,128)(2,1)} %reshape.146), calls=%async_computation | async-start | bytes 1048576 | tf_op jit(solution)/shard_map/all_to_all | solution.py:33
  257.6 23.2 %copy-start.2 = (bf16[2048,128]{1,0:T(8,128)(2,1)S(1)}, bf16[2048,128]{1,0:T(8,128)(2,1)}, u32[]{:S(2)}) copy-start(bf16[2048,128]{1,0:T(8,128)(2,1)} %param.19) | copy-start | bytes 1572868
  259.0 22.1 %copy-start.4 = (bf16[2048,128]{1,0:T(8,128)(2,1)S(1)}, bf16[2048,128]{1,0:T(8,128)(2,1)}, u32[]{:S(2)}) copy-start(bf16[2048,128]{1,0:T(8,128)(2,1)} %param.20) | copy-start | bytes 1572868
Sparse Core Ops, SparseCore 0:
  11.6 66.0 all-gather.7
  80.7 60.2 all-gather.5
where the time goes:
time: 302 us; the launch traced here: 300 us
  waiting for transfers between devices  104 us (34%)
  blocking collectives  75.9 us (25%)
  matrix products  55.5 us (18%)
  starting transfers between devices  30 us (10%)
  between operations  14.4 us (5%)
  local copies, waits for them, and re-layouts  11 us (4%)
  other arithmetic  8.44 us (3%)
    all_gather x2, waiting for transfers between devices, in_one_piece(): lax.all_gather(both, axis, axis=dim, tiled=True)  76.8 us
    all_gather x2, blocking collectives, in_one_piece(): lax.all_gather(both, axis, axis=dim, tiled=True)  55.1 us
    all_to_all x2, waiting for transfers between devices, sum_at_owner(): lax.all_to_all(blocks, axis, split_axis=0, concat_axis=0, tiled=True)  27 us
    all_to_all x2, starting transfers between devices, sum_at_owner(): lax.all_to_all(blocks, axis, split_axis=0, concat_axis=0, tiled=True)  23.1 us
    all_gather x2, blocking collectives, whole_of(): result = lax.all_gather(result, axes[number], axis=dim, tiled=True)  20.8 us
    dot_general x8, matrix products, collect_one_block(): jnp.einsum('ihj,ihd->jd', score_grad, query_block, preferred_element_type...  11.1 us
    dot_general x8, matrix products, collect_one_block(): jnp.einsum('ihj,ihd->jd', prob_rows.astype(jnp.bfloat16), grad_block, pre...  8.91 us
    dot_general x8, matrix products, collect_one_block(): jnp.einsum('ihd,jd->ihj', query_block, key_group, preferred_element_type=...  8.81 us
  transfers between devices with their start and end apart: 5, of which 4 were waited for; matrix products, arithmetic and copies ran while one was open for 23% of the time, Pallas kernels for 0%

commit v1 on v0

v1 whole, which is shorter than its diff:
```python
import functools
import math

import jax
import jax.numpy as jnp
from jax import lax
from jax.experimental import pallas as pl
from jax.experimental.pallas import tpu as pltpu
from jax.sharding import Mesh
from jax.sharding import PartitionSpec as P

HEAD = 128
NORM_EPS = 1e-06
INV_ROOT = HEAD ** (-0.5)
LOG2E = math.log2(math.e)
F32, BF16 = jnp.float32, jnp.bfloat16
NN = (((1,), (0,)), ((), ()))
NT = (((1,), (1,)), ((), ()))
TN = (((0,), (0,)), ((), ()))
SHAPE = {"y": 4, "x": 4, "c": 2}


def dot(a, b, dims):
    return lax.dot_general(a, b, dims, preferred_element_type=F32)


def norm_rows(src, dst, gain):
    rows, step = src.shape[0], 16

    def one(k, carry):
        at = pl.ds(pl.multiple_of(k * step, step), step)
        v = src[at, :].astype(F32)
        r = lax.rsqrt(jnp.mean(v * v, axis=1, keepdims=True) + NORM_EPS)
        dst[at, :] = (v * r * gain[...]).astype(BF16)
        return carry

    lax.fori_loop(0, rows // step, one, 0)


def norm_back(rows, gain, upstream):
    r = lax.rsqrt(jnp.mean(rows * rows, axis=1, keepdims=True) + NORM_EPS)
    unit = rows * r
    pulled = upstream * gain
    return (r * (pulled - unit * jnp.mean(pulled * unit, axis=1, keepdims=True))).astype(BF16)


def wait_bytes(ref, sem):
    pltpu.make_async_copy(ref, ref, sem).wait()


def kernel(
    dims, tgt_h, src_h, cot_h, tg_h, sg_h, wq_h, wk_h, wv_h, wo_h,
    gt_o, gs_o, go_o,
    srcb, swin, sn, tgtb, twin, tn, cotb, tgb, sgb, wqb, wkv, wob,
    kv, qg, est, pgt, ds_b, pr_b, stat, gqt, att,
    ys, yr, gkv, ps, pr, xs, xr, xown, kvs, zk, zr,
    pmat, tpo, tpr, tmine, ts, tr, gos, gor,
    ld, kv_r, kvp_r, qg_r, st_r, y_r, ps_r, x_r, zk_r, tp_r, t_r, go_r,
    kv_s, kvp_s, qg_s, st_s, y_s, ps_s, x_s, zk_s, tp_s, t_s, go_s,
):
    ny, nx, nz, gsz, rt, rs, win = dims
    ns = ny * nx
    y, x, z, c = (lax.axis_index(a) for a in ("y", "x", "z", "c"))
    o = 1 - c
    s_me = y * nx + x
    half = kv.shape[2]
    rows = tgtb.shape[0]
    width = tgtb.shape[1]

    barrier = pltpu.get_barrier_semaphore()
    peers = [{"c": o}]
    for dy in range(ny):
        for dx in range(nx):
            if dy or dx:
                peers.append({"y": lax.rem(y + dy, ny), "x": lax.rem(x + dx, nx)})
    for dz in range(1, nz):
        for cc in (c, o):
            peers.append({"z": lax.rem(z + dz, nz), "c": cc})
    for peer in peers:
        pl.semaphore_signal(barrier, inc=1, device_id=peer, device_id_type=pl.DeviceIdType.MESH)

    def load(k, a, b):
        d = pltpu.make_async_copy(a, b, ld.at[k])
        d.start()
        return d

    t_me = 2 * z + c
    w0 = pl.multiple_of(lax.div(rs * t_me, 8) * 8, 8)
    l_src = load(0, src_h.at[pl.ds(pl.multiple_of(c * half, half), half), :], srcb)
    l_sg = load(1, sg_h, sgb)
    l_wk = load(2, wk_h, wkv.at[:, pl.ds(0, HEAD)])
    l_wv = load(3, wv_h, wkv.at[:, pl.ds(HEAD, HEAD)])
    l_tgt = load(4, tgt_h, tgtb)
    l_tg = load(5, tg_h, tgb)
    l_wq = load(6, wq_h, wqb)
    l_cot = load(7, cot_h, cotb)
    l_wo = load(8, wo_h, wob)
    l_swin = load(9, src_h.at[pl.ds(w0, win), :], swin)
    l_twin = load(10, tgt_h.at[pl.ds(pl.multiple_of(2 * rt * z, 2 * rt), 2 * rt), :], twin)

    def send(a, b, s_sem, r_sem, to):
        d = pltpu.make_async_remote_copy(
            src_ref=a, dst_ref=b, send_sem=s_sem, recv_sem=r_sem,
            device_id=to, device_id_type=pl.DeviceIdType.MESH,
        )
        d.start()
        return d

    l_src.wait()
    l_sg.wait()
    norm_rows(srcb, sn, sgb)
    l_wk.wait()
    l_wv.wait()
    kv[0, c] = dot(sn[...], wkv[...], NN).astype(BF16)
    pl.semaphore_wait(barrier, len(peers))
    sends = []
    for d in range(1, nx):
        sends.append(send(kv.at[0, c], kv.at[d, c], kv_s.at[d], kv_r.at[d], {"x": lax.rem(x + d, nx)}))
    sends.append(send(kv.at[0, c], kv.at[0, c], kvp_s.at[0], kvp_r.at[0], {"c": o}))

    l_tgt.wait()
    l_tg.wait()
    norm_rows(tgtb, tn, tgb)
    l_wq.wait()
    qg[0, :, pl.ds(0, HEAD)] = dot(tn[...], wqb[...], NN).astype(BF16)
    l_cot.wait()
    l_wo.wait()
    qg[0, :, pl.ds(HEAD, HEAD)] = dot(cotb[...], wob[...], NT).astype(BF16)
    for d in range(1, ny):
        sends.append(send(qg.at[0], qg.at[d], qg_s.at[d], qg_r.at[d], {"y": lax.rem(y + d, ny)}))

    for d in range(1, ny):
        wait_bytes(qg.at[d], qg_r.at[d])
    q_all = qg[:, :, pl.ds(0, HEAD)].reshape(ny * rows, HEAD)
    g_all = qg[:, :, pl.ds(HEAD, HEAD)].reshape(ny * rows, HEAD)
    tot = jnp.zeros((1, ny * rows), F32)
    tilt = jnp.zeros((1, ny * rows), F32)

    def unit(d, h, tot, tilt):
        e = jnp.exp2(dot(kv[d, h, :, pl.ds(0, HEAD)], q_all, NT) * (INV_ROOT * LOG2E))
        g = dot(kv[d, h, :, pl.ds(HEAD, HEAD)], g_all, NT)
        est[d, h] = e
        pgt[d, h] = g
        return tot + jnp.sum(e, axis=0, keepdims=True), tilt + jnp.sum(e * g, axis=0, keepdims=True)

    tot, tilt = unit(0, c, tot, tilt)
    for d in range(1, nx):
        wait_bytes(kv.at[d, c], kv_r.at[d])
        sends.append(send(kv.at[d, c], kv.at[d, c], kvp_s.at[d], kvp_r.at[d], {"c": o}))
        wait_bytes(kv.at[d - 1, o], kvp_r.at[d - 1])
        tot, tilt = unit(d - 1, o, tot, tilt)
        tot, tilt = unit(d, c, tot, tilt)
    wait_bytes(kv.at[nx - 1, o], kvp_r.at[nx - 1])
    tot, tilt = unit(nx - 1, o, tot, tilt)

    for e in range(ny):
        stat[0, e, 0:1, :] = tot[:, e * rows:(e + 1) * rows]
        stat[0, e, 1:2, :] = tilt[:, e * rows:(e + 1) * rows]
    for d in range(1, ny):
        sends.append(send(stat.at[0], stat.at[d], st_s.at[d], st_r.at[d], {"y": lax.rem(y + d, ny)}))
    for d in range(1, ny):
        wait_bytes(stat.at[d], st_r.at[d])
    tots, deltas = [], []
    for e in range(ny):
        both = stat[0, e]
        for d in range(1, ny):
            both = both + stat[d, (e - d) % ny]
        tots.append(1.0 / both[0:1, :])
        deltas.append(both[1:2, :] / both[0:1, :])
    inv_total = jnp.concatenate(tots, axis=1)
    delta = jnp.concatenate(deltas, axis=1)

    gq_sum, at_sum = None, None
    for d in range(nx):
        for h in range(2):
            p = est[d, h] * inv_total
            dsv = (p * (pgt[d, h] - delta)).astype(BF16)
            p = p.astype(BF16)
            pr_b[d, h] = p
            ds_b[d, h] = dsv
            gq_one = dot(kv[d, h, :, pl.ds(0, HEAD)], dsv, TN)
            at_one = dot(kv[d, h, :, pl.ds(HEAD, HEAD)], p, TN)
            gq_sum = gq_one if gq_sum is None else gq_sum + gq_one
            at_sum = at_one if at_sum is None else at_sum + at_one
    gqt[...] = gq_sum[:, 0:rows]
    att[...] = at_sum[:, 0:rows]
    for e in range(1, ny):
        ys[e, 0] = gq_sum[:, e * rows:(e + 1) * rows].astype(BF16)
        ys[e, 1] = at_sum[:, e * rows:(e + 1) * rows].astype(BF16)
        sends.append(send(ys.at[e], yr.at[e], y_s.at[e], y_r.at[e], {"y": lax.rem(y + ny - e, ny)}))

    order = [d for d in (2, 1, 3, 0) if d < nx]
    for d in order:
        for h in range(2):
            at = pl.ds(h * half, half)
            gkv[0, d, at, :] = dot(ds_b[d, h], q_all, NN) * INV_ROOT
            gkv[1, d, at, :] = dot(pr_b[d, h], g_all, NN)
        ps[d] = gkv[o, d].astype(BF16)
        sends.append(send(ps.at[d], pr.at[d], ps_s.at[d], ps_r.at[d], {"c": o}))
    for d in order:
        wait_bytes(pr.at[d], ps_r.at[d])
        mine = gkv[c, d] + pr[d].astype(F32)
        if d:
            xs[d] = mine.astype(BF16)
            sends.append(send(xs.at[d], xr.at[d], x_s.at[d], x_r.at[d], {"x": lax.rem(x + nx - d, nx)}))
        else:
            xown[...] = mine

    for e in range(1, ny):
        wait_bytes(yr.at[e], y_r.at[e])
    gq = gqt[...]
    av = att[...]
    for e in range(1, ny):
        gq = gq + yr[e, 0].astype(F32)
        av = av + yr[e, 1].astype(F32)
    gq = (gq * INV_ROOT).T.astype(BF16)
    pmat[...] = dot(gq, wqb[...], NT)
    for k in range(nz):
        a = pmat[pl.ds(2 * rt * k, rt), :]
        b = pmat[pl.ds(2 * rt * k + rt, rt), :]
        tmine[k] = jnp.where(c == 0, a, b)
        tpo[k] = jnp.where(c == 0, b, a).astype(BF16)
    sends.append(send(tpo, tpr, tp_s, tp_r, {"c": o}))
    go = dot(av.astype(BF16), cotb[...], NN)
    wc = width // ns
    for k in range(ns):
        gos[k] = go[:, k * wc:(k + 1) * wc].astype(BF16)
    for dy in (2, 1, 3, 0):
        for dx in (2, 1, 3, 0):
            if dy < ny and dx < nx and (dy or dx):
                py, px = lax.rem(y + dy, ny), lax.rem(x + dx, nx)
                send(gos.at[py * nx + px], gor.at[s_me], go_s, go_r, {"y": py, "x": px})
    wait_bytes(tpr, tp_r)
    ts[...] = (tmine[...] + tpr[...].astype(F32)).astype(BF16)
    far = sorted(range(1, nz), key=lambda k: -min(k, nz - k))
    for dz in far:
        pz = lax.rem(z + dz, nz)
        send(ts.at[pz], tr.at[z], t_s, t_r, {"z": pz})

    ksum = xown[...]
    for d in range(1, nx):
        wait_bytes(xr.at[d], x_r.at[d])
        ksum = ksum + xr[d].astype(F32)
    kvs[...] = ksum
    for k in range(nz):
        for cc in range(2):
            zk[2 * k + cc] = kvs[pl.ds(2 * rs * k + rs * cc, rs), :].astype(BF16)
    for dz in far:
        pz = lax.rem(z + dz, nz)
        for cc in (c, o):
            send(zk.at[2 * pz + cc], zr.at[t_me], zk_s, zk_r, {"z": pz, "c": cc})
    send(zk.at[2 * z + o], zr.at[t_me], zk_s, zk_r, {"c": o})
    zr[t_me] = zk[t_me]
    gor[s_me] = gos[s_me]
    tr[z] = ts[z]

    l_twin.wait()
    wait_bytes(tr.at[pl.ds(0, nz - 1)], t_r)
    up = jnp.sum(tr[...].astype(F32), axis=0)
    tw = twin[...].astype(F32)
    tw = jnp.where(c == 0, tw[0:rt, :], tw[rt:2 * rt, :])
    gt_o[...] = norm_back(tw, tgb[...], up)

    wait_bytes(gor.at[pl.ds(0, ns - 1)], go_r)
    go_o[...] = jnp.sum(gor[...].astype(F32), axis=0).astype(BF16)

    l_swin.wait()
    row_at = lax.broadcasted_iota(jnp.int32, (rs, win), 0) + (rs * t_me - w0)
    pick = (lax.broadcasted_iota(jnp.int32, (rs, win), 1) == row_at).astype(F32).astype(BF16)
    sw = dot(pick, swin[...], NN)
    wait_bytes(zr.at[pl.ds(0, 2 * nz - 1)], zk_r)
    both = [zr[0].astype(F32), zr[1].astype(F32)]
    for k in range(2, 2 * nz):
        both[k % 2] = both[k % 2] + zr[k].astype(F32)
    both = jnp.concatenate(both, axis=1).astype(BF16)
    gs_o[...] = norm_back(sw, sgb[...], dot(both, wkv[...], NT))

    for d in sends:
        d.wait_send()
    wait_bytes(gos.at[pl.ds(0, ns - 1)], go_s)
    wait_bytes(ts.at[pl.ds(0, nz - 1)], t_s)
    wait_bytes(zk.at[pl.ds(0, 2 * nz - 1)], zk_s)


def on_device(shape, target, source, cotangent, target_gain, source_gain, w_query, w_key, w_value, w_out):
    ny, nx, nz = shape
    rows, width = target.shape
    srows = source.shape[0]
    half = srows // 2
    rt, rs = rows // (2 * nz), srows // (2 * nz)
    win = rs if rs % 8 == 0 else rs + 4
    ns = ny * nx
    wide = ny * rows
    vm = pltpu.VMEM
    sem = pltpu.SemaphoreType.DMA
    scratch = [
        vm((half, width), BF16), vm((win, width), BF16), vm((half, width), BF16),
        vm((rows, width), BF16), vm((2 * rt, width), BF16), vm((rows, width), BF16),
        vm((rows, width), BF16), vm((1, width), F32), vm((1, width), F32),
        vm((width, HEAD), BF16), vm((width, 2 * HEAD), BF16), vm((HEAD, width), BF16),
        vm((nx, 2, half, 2 * HEAD), BF16), vm((ny, rows, 2 * HEAD), BF16),
        vm((nx, 2, half, wide), F32), vm((nx, 2, half, wide), F32),
        vm((nx, 2, half, wide), BF16), vm((nx, 2, half, wide), BF16),
        vm((ny, ny, 2, rows), F32), vm((HEAD, rows), F32), vm((HEAD, rows), F32),
        vm((ny, 2, HEAD, rows), BF16), vm((ny, 2, HEAD, rows), BF16),
        vm((2, nx, srows, HEAD), F32), vm((nx, srows, HEAD), BF16), vm((nx, srows, HEAD), BF16),
        vm((nx, srows, HEAD), BF16), vm((nx, srows, HEAD), BF16), vm((srows, HEAD), F32),
        vm((srows, HEAD), F32), vm((2 * nz, rs, HEAD), BF16), vm((2 * nz, rs, HEAD), BF16),
        vm((rows, width), F32), vm((nz, rt, width), BF16), vm((nz, rt, width), BF16),
        vm((nz, rt, width), F32), vm((nz, rt, width), BF16), vm((nz, rt, width), BF16),
        vm((ns, HEAD, width // ns), BF16), vm((ns, HEAD, width // ns), BF16),
        sem((11,)), sem((nx,)), sem((nx,)), sem((ny,)), sem((ny,)), sem((ny,)), sem((nx,)), sem((nx,)),
        sem, sem, sem, sem,
        sem((nx,)), sem((nx,)), sem((ny,)), sem((ny,)), sem((ny,)), sem((nx,)), sem((nx,)),
        sem, sem, sem, sem,
    ]
    any_spec = pl.BlockSpec(memory_space=pl.ANY)
    vm_spec = pl.BlockSpec(memory_space=pltpu.VMEM)
    return pl.pallas_call(
        functools.partial(kernel, (ny, nx, nz, 0, rt, rs, win)),
        out_shape=(
            jax.ShapeDtypeStruct((rt, width), BF16),
            jax.ShapeDtypeStruct((rs, width), BF16),
            jax.ShapeDtypeStruct((HEAD, width // ns), BF16),
        ),
        in_specs=[any_spec] * 9,
        out_specs=(vm_spec,) * 3,
        scratch_shapes=scratch,
        compiler_params=pltpu.CompilerParams(
            collective_id=0, has_side_effects=True, vmem_limit_bytes=67043328
        ),
    )(
        target, source, cotangent, target_gain.reshape(1, width), source_gain.reshape(1, width),
        w_query, w_key, w_value, w_out,
    )


def solution(mesh, ny=4, nx=4):
    nz = mesh.shape["tp"] // 2
    split = Mesh(mesh.devices.reshape(ny, nx, nz, 2), ("y", "x", "z", "c"))
    sp, tp, every = ("y", "x"), ("z", "c"), ("y", "x", "z", "c")
    in_specs = (P(sp, None), P(sp, None), P(sp, None), P(), P(), P(None, tp), P(), P(), P(tp, None))
    out_specs = (P(every, None), P(every, None), P(tp, sp))
    return jax.shard_map(
        functools.partial(on_device, (ny, nx, nz)),
        mesh=split, in_specs=in_specs, out_specs=out_specs, check_vma=False,
    )
```

time: 302 us -> 64 us (0.21)
  waiting for transfers between devices: 104 us -> 0 us
  blocking collectives: 75.9 us -> 0 us
  Pallas kernels: 0 us -> 58.9 us
  matrix products: 55.5 us -> 0 us
  starting transfers between devices: 30 us -> 0 us
  between operations: 14.4 us -> 0.64 us
  other arithmetic: 8.44 us -> 0 us
  local copies, waits for them, and re-layouts: 11 us -> 4.18 us
    all_gather x2 -> x0, waiting for transfers between devices: 76.8 us -> none  [in_one_piece(): lax.all_gather(both, axis, axis=dim, tiled=True)]
    all_gather x4 -> x0, blocking collectives: 75.9 us -> none  [the longest x2 55.1 us: in_one_piece(): lax.all_gather(both, axis, axis=dim, tiled=True)]
    pallas_call x0 -> x1, Pallas kernels: none -> 58.9 us  [on_device(): pl.pallas_call(functools.partial(kernel, (ny, nx, nz, 0, rt, rs, win)), o...]
    dot_general x56 -> x0, matrix products: 55.5 us -> none  [the longest x8 11.1 us: collect_one_block(): jnp.einsum('ihj,ihd->jd', score_grad, query_block, preferred_element_type...]
    all_to_all x3 -> x0, starting transfers between devices: 29.9 us -> none  [the longest x2 23.1 us: sum_at_owner(): lax.all_to_all(blocks, axis, split_axis=0, concat_axis=0, tiled=True)]
    all_to_all x3 -> x0, waiting for transfers between devices: 27 us -> none  [the longest x2 27 us: sum_at_owner(): lax.all_to_all(blocks, axis, split_axis=0, concat_axis=0, tiled=True)]
    split x4 -> x0, local copies, waits for them, and re-layouts: 5.58 us -> none  [in_one_piece(): jnp.split(lax.all_gather(both, axis, axis=dim, tiled=True), ends, axis=al...]
    reduce_sum x7 -> x0, other arithmetic: 4.54 us -> none  [the longest x2 2.37 us: normed(): jnp.mean(rows_wide * rows_wide, axis=1, keepdims=True) + NORM_EPS]
  transfers between devices with their start and end apart: 5 -> 0, of which waited for: 4 -> 0; matrix products, arithmetic and copies ran while one was open for 23% -> 0% of each run, Pallas kernels for 0% -> 0%
where the time goes in v1:
time: 64 us; the launch traced here: 63.7 us
  Pallas kernels  58.9 us (92%)
  local copies, waits for them, and re-layouts  4.18 us (7%)
  between operations  0.64 us (1%)
    pallas_call x1, Pallas kernels, on_device(): pl.pallas_call(functools.partial(kernel, (ny, nx, nz, 0, rt, rs, win)), o...  58.9 us
    unnamed x3, local copies, waits for them, and re-layouts  4.18 us

profile of v1, /device:TPU:1, one launch (start us, length us, event | category | flops | bytes accessed | tf_op | source)
XLA Modules:
  0.0 63.7 jit_solution(17945043540041184611)
XLA Ops:
  0.6 58.9 %shard_map.112 = (bf16[4,2048]{1,0:T(4,128)(2,1)}, bf16[12,2048]{1,0:T(8,128)(2,1)}, bf16[128,128]{1,0:T(8,128)(2,1)}) custom-call(bf16[128,2048]{1,0:T(8,128)(2,1)} %tgt_h.1, bf16[384,2048]{1,0:T(8,128)(2,1)} %src_h.1, bf16[128,2048]{1,0:T(8,128)(2,1)} %cot_h.1, f32[1,2048]{1,0:T(1,128)} %bitcast.2, f32[1,2048]{1,0:T(1,128)} %bitcast.3, ...), custom_call_target="tpu_custom_call" | custom-call | tf_op jit(solution)/shard_map/pallas_call | solution.py:319
  59.5 1.3 %copy.15 = bf16[4,2048]{1,0:T(4,128)(2,1)} copy(bf16[4,2048]{1,0:T(4,128)(2,1)} %get-tuple-element.6) | data formatting | bytes 32768
  60.9 1.5 %copy.16 = bf16[12,2048]{1,0:T(8,128)(2,1)} copy(bf16[12,2048]{1,0:T(8,128)(2,1)} %get-tuple-element.7) | data formatting | bytes 98304
  62.3 1.4 %copy.17 = bf16[128,128]{1,0:T(8,128)(2,1)} copy(bf16[128,128]{1,0:T(8,128)(2,1)} %get-tuple-element.8) | data formatting | bytes 65536

commit v2 on v1

v2 whole, which is shorter than its diff:
```python
import functools
import math

import jax
import jax.numpy as jnp
from jax import lax
from jax.experimental import pallas as pl
from jax.experimental.pallas import tpu as pltpu
from jax.sharding import Mesh
from jax.sharding import PartitionSpec as P

HEAD = 128
NORM_EPS = 1e-06
INV_ROOT = HEAD ** (-0.5)
LOG2E = math.log2(math.e)
F32, BF16 = jnp.float32, jnp.bfloat16
NN = (((1,), (0,)), ((), ()))
NT = (((1,), (1,)), ((), ()))
TN = (((0,), (0,)), ((), ()))
SHAPE = {"y": 4, "x": 4, "c": 2}


def dot(a, b, dims):
    return lax.dot_general(a, b, dims, preferred_element_type=F32)


def norm_rows(src, dst, gain):
    rows, step = src.shape[0], 16

    def one(k, carry):
        at = pl.ds(pl.multiple_of(k * step, step), step)
        v = src[at, :].astype(F32)
        r = lax.rsqrt(jnp.mean(v * v, axis=1, keepdims=True) + NORM_EPS)
        dst[at, :] = (v * r * gain[...]).astype(BF16)
        return carry

    lax.fori_loop(0, rows // step, one, 0, unroll=4)


def norm_back(rows, gain, upstream):
    r = lax.rsqrt(jnp.mean(rows * rows, axis=1, keepdims=True) + NORM_EPS)
    unit = rows * r
    pulled = upstream * gain
    return (r * (pulled - unit * jnp.mean(pulled * unit, axis=1, keepdims=True))).astype(BF16)


def wait_bytes(ref, sem):
    pltpu.make_async_copy(ref, ref, sem).wait()


def kernel(
    dims, tgt_h, src_h, cot_h, tg_h, sg_h, wq_h, wk_h, wv_h, wo_h,
    gt_o, gs_o, go_o,
    srcb, swin, sn, tgtb, twin, tn, cotb, tgb, sgb, wkv, wob,
    kv, qg, est, pgt, e_b, t_b, stat, aw, tk,
    ys, yr, gkv, ps, pr, xs, xr, xown, kvs, zk, zr,
    wq4, gqo, gqi, pmat, ts, tr, gos, gor,
    ld, kv_r, kvp_r, qg_r, st_r, y_r, ps_r, x_r, zk_r, wq_r, gq_r, t_r, go_r,
    kv_s, kvp_s, qg_s, st_s, y_s, ps_s, x_s, zk_s, wq_s, gq_s, t_s, go_s,
    up_1, up_2, up_4,
):
    ny, nx, nz, gsz, rt, rs, win = dims
    ns = ny * nx
    y, x, z, c = (lax.axis_index(a) for a in ("y", "x", "z", "c"))
    o = 1 - c
    s_me = y * nx + x
    zo = z + 1 - 2 * lax.rem(z, 2)
    zf = lax.rem(z - 1 + 2 * lax.rem(z, 2) + nz, nz)
    mem = 2 * lax.rem(z, 2) + c
    half = kv.shape[2]
    rows = tgtb.shape[0]
    width = tgtb.shape[1]

    barrier = pltpu.get_barrier_semaphore()

    def signal(sem, to):
        pl.semaphore_signal(sem, inc=1, device_id=to, device_id_type=pl.DeviceIdType.MESH)

    def beside(k):
        return [lax.rem(z + k, nz), lax.rem(z + nz - k, nz)] if 2 * k < nz else [lax.rem(z + k, nz)]

    peers = [{"c": o}]
    for dy in range(ny):
        for dx in range(nx):
            if dy or dx:
                peers.append({"y": lax.rem(y + dy, ny), "x": lax.rem(x + dx, nx)})
    for dy in range(ny):
        py = lax.rem(y + dy, ny)
        peers.extend([{"y": py, "z": zo, "c": c}, {"y": py, "z": zo, "c": o}])
        if dy:
            peers.append({"y": py, "c": o})
    if nz > 2:
        peers.extend([{"z": zf, "c": c}, {"z": zf, "c": o}])
    for peer in peers:
        signal(barrier, peer)

    def load(k, a, b):
        d = pltpu.make_async_copy(a, b, ld.at[k])
        d.start()
        return d

    t_me = 2 * z + c
    w0 = pl.multiple_of(lax.div(rs * t_me, 8) * 8, 8)
    l_tgt = load(4, tgt_h, tgtb)
    l_tg = load(5, tg_h, tgb)
    l_wq = load(6, wq_h, wq4.at[mem])
    l_cot = load(7, cot_h, cotb)
    l_wo = load(8, wo_h, wob)
    l_src = load(0, src_h.at[pl.ds(pl.multiple_of(c * half, half), half), :], srcb)
    l_sg = load(1, sg_h, sgb)
    l_wk = load(2, wk_h, wkv.at[:, pl.ds(0, HEAD)])
    l_wv = load(3, wv_h, wkv.at[:, pl.ds(HEAD, HEAD)])
    l_swin = load(9, src_h.at[pl.ds(w0, win), :], swin)
    l_twin = load(10, tgt_h.at[pl.ds(pl.multiple_of(2 * rt * z, 2 * rt), 2 * rt), :], twin)

    def send(a, b, s_sem, r_sem, to):
        d = pltpu.make_async_remote_copy(
            src_ref=a, dst_ref=b, send_sem=s_sem, recv_sem=r_sem,
            device_id=to, device_id_type=pl.DeviceIdType.MESH,
        )
        d.start()
        return d

    l_tgt.wait()
    l_tg.wait()
    norm_rows(tgtb, tn, tgb)
    l_wq.wait()
    qg[0, :, pl.ds(0, HEAD)] = dot(tn[...], wq4[mem], NN).astype(BF16)
    l_cot.wait()
    l_wo.wait()
    qg[0, :, pl.ds(HEAD, HEAD)] = dot(cotb[...], wob[...], NT).astype(BF16)
    pl.semaphore_wait(barrier, len(peers))
    sends = []
    x_order = [d for d in (2, 1, 3) if d < nx]
    y_order = [d for d in (2, 1, 3) if d < ny]
    for d in y_order:
        sends.append(send(qg.at[0], qg.at[d], qg_s.at[d], qg_r.at[d], {"y": lax.rem(y + d, ny)}))
    for pz in beside(1):
        signal(up_1, {"z": pz})
    sends.append(send(wq4.at[mem], wq4.at[mem], wq_s.at[0], wq_r.at[0], {"z": zo}))
    sends.append(send(wq4.at[mem], wq4.at[mem], wq_s.at[1], wq_r.at[1], {"c": o}))

    l_src.wait()
    l_sg.wait()
    norm_rows(srcb, sn, sgb)
    l_wk.wait()
    l_wv.wait()
    kv[0, c] = dot(sn[...], wkv[...], NN).astype(BF16)
    for d in x_order:
        sends.append(send(kv.at[0, c], kv.at[d, c], kv_s.at[d], kv_r.at[d], {"x": lax.rem(x + d, nx)}))
    sends.append(send(kv.at[0, c], kv.at[0, c], kvp_s.at[0], kvp_r.at[0], {"c": o}))
    pl.semaphore_wait(up_1, len(beside(1)))
    for pz in beside(2):
        signal(up_2, {"z": pz})

    for d in range(1, ny):
        wait_bytes(qg.at[d], qg_r.at[d])
    pl.semaphore_wait(up_2, len(beside(2)))
    for pz in beside(4):
        signal(up_4, {"z": pz})
    q_all = qg[:, :, pl.ds(0, HEAD)].reshape(ny * rows, HEAD)
    g_all = qg[:, :, pl.ds(HEAD, HEAD)].reshape(ny * rows, HEAD)
    tot = jnp.zeros((1, ny * rows), F32)
    tilt = jnp.zeros((1, ny * rows), F32)

    def unit(d, h, tot, tilt):
        key, val = kv[d, h, :, pl.ds(0, HEAD)], kv[d, h, :, pl.ds(HEAD, HEAD)]
        e = jnp.exp2(dot(key, q_all, NT) * (INV_ROOT * LOG2E))
        g = dot(val, g_all, NT)
        t = e * g
        est[d, h] = e
        pgt[d, h] = g
        e_b[d, h] = e.astype(BF16)
        t_b[d, h] = t.astype(BF16)
        return tot + jnp.sum(e, axis=0, keepdims=True), tilt + jnp.sum(t, axis=0, keepdims=True)

    def unit_sums(d, h, first):
        both = dot(kv[d, h], e_b[d, h], TN)
        one = dot(kv[d, h, :, pl.ds(0, HEAD)], t_b[d, h], TN)
        aw[...] = both if first else aw[...] + both
        tk[...] = one if first else tk[...] + one

    x_seen = [d for d in (1, 3, 2) if d < nx]
    tot, tilt = unit(0, c, tot, tilt)
    unit_sums(0, c, True)
    before = 0
    for d in x_seen:
        wait_bytes(kv.at[d, c], kv_r.at[d])
        sends.append(send(kv.at[d, c], kv.at[d, c], kvp_s.at[d], kvp_r.at[d], {"c": o}))
        wait_bytes(kv.at[before, o], kvp_r.at[before])
        tot, tilt = unit(before, o, tot, tilt)
        unit_sums(before, o, False)
        tot, tilt = unit(d, c, tot, tilt)
        if d != x_seen[-1]:
            unit_sums(d, c, False)
        before = d
    wait_bytes(kv.at[before, o], kvp_r.at[before])
    tot, tilt = unit(before, o, tot, tilt)

    for e in range(ny):
        stat[0, e, 0:1, :] = tot[:, e * rows:(e + 1) * rows]
        stat[0, e, 1:2, :] = tilt[:, e * rows:(e + 1) * rows]
    for d in y_order:
        sends.append(send(stat.at[0], stat.at[d], st_s.at[d], st_r.at[d], {"y": lax.rem(y + d, ny)}))
    unit_sums(before, c, False)
    unit_sums(before, o, False)
    for e in y_order:
        ys[e] = aw[pl.ds(HEAD, HEAD), pl.ds(e * rows, rows)].astype(BF16)
        sends.append(send(ys.at[e], yr.at[e], y_s.at[e], y_r.at[e], {"y": lax.rem(y + ny - e, ny)}))
    for d in range(1, ny):
        wait_bytes(stat.at[d], st_r.at[d])
    tots, deltas = [], []
    for e in range(ny):
        both = stat[0, e]
        for d in range(1, ny):
            both = both + stat[d, (e - d) % ny]
        tots.append(1.0 / both[0:1, :])
        deltas.append(both[1:2, :] / both[0:1, :])
    inv_total = jnp.concatenate(tots, axis=1)
    delta = jnp.concatenate(deltas, axis=1)

    gq = ((tk[...] - delta * aw[pl.ds(0, HEAD), :]) * (inv_total * INV_ROOT)).T.astype(BF16)
    quarter = rows // 4
    for e in range(ny):
        for k in range(4):
            gqo[4 * e + k] = gq[e * rows + k * quarter:e * rows + (k + 1) * quarter, :]
    for e in y_order + [0]:
        py = lax.rem(y + ny - e, ny)
        for step in (2, 3, 1, 0):
            if e or step:
                pz = zo if step > 1 else z
                pc = o if step % 2 else c
                to = 2 * lax.rem(pz, 2) + pc
                send(gqo.at[4 * e + to], gqi.at[4 * e + mem], gq_s, gq_r, {"y": py, "z": pz, "c": pc})
    gqi[mem] = gqo[mem]
    scale = jnp.broadcast_to(inv_total, (8, ny * rows)).T[:, 0:1]
    q_div = (q_all.astype(F32) * scale).astype(BF16)
    g_div = (g_all.astype(F32) * scale).astype(BF16)
    order = [d for d in (2, 1, 3, 0) if d < nx]
    for d in order:
        for h in range(2):
            at = pl.ds(h * half, half)
            dsv = (est[d, h] * (pgt[d, h] - delta)).astype(BF16)
            gkv[0, d, at, :] = dot(dsv, q_div, NN) * INV_ROOT
            gkv[1, d, at, :] = dot(e_b[d, h], g_div, NN)
        ps[d] = gkv[o, d].astype(BF16)
        sends.append(send(ps.at[d], pr.at[d], ps_s.at[d], ps_r.at[d], {"c": o}))
    for d in order:
        wait_bytes(pr.at[d], ps_r.at[d])
        mine = gkv[c, d] + pr[d].astype(F32)
        if d:
            xs[d] = mine.astype(BF16)
            sends.append(send(xs.at[d], xr.at[d], x_s.at[d], x_r.at[d], {"x": lax.rem(x + nx - d, nx)}))
        else:
            xown[...] = mine

    wait_bytes(wq4.at[0], wq_r.at[0])
    mem_z = 2 * lax.rem(zo, 2) + c
    sends.append(send(wq4.at[mem_z], wq4.at[mem_z], wq_s.at[2], wq_r.at[2], {"c": o}))
    wait_bytes(gqi.at[pl.ds(0, 4 * ny - 1)], gq_r)
    wait_bytes(wq4.at[0], wq_r.at[1])
    wait_bytes(wq4.at[0], wq_r.at[2])
    up = None
    for k in range(4):
        one = gqi[k].astype(F32)
        for e in range(1, ny):
            one = one + gqi[4 * e + k].astype(F32)
        one = dot(one.astype(BF16), wq4[k], NT)
        up = one if up is None else up + one
    pmat[...] = up
    pieces = quarter // rt
    for k in range(pieces):
        ts[k] = pmat[pl.ds(rt * k, rt), :].astype(BF16)
    pl.semaphore_wait(up_4, len(beside(4)))
    pair = lax.div(z, 2)
    per = pieces // 2
    for k in range(pieces):
        pz, pc = per * mem + k // 2, k % 2
        mine = jnp.logical_and(pz == z, pc == c)

        @pl.when(jnp.logical_not(mine))
        def _():
            send(ts.at[k], tr.at[pair], t_s, t_r, {"z": pz, "c": pc})

        @pl.when(mine)
        def _():
            tr[pair] = ts[k]

    for e in range(1, ny):
        wait_bytes(yr.at[e], y_r.at[e])
    av = aw[pl.ds(HEAD, HEAD), pl.ds(0, rows)]
    for e in range(1, ny):
        av = av + yr[e].astype(F32)
    go = dot((av * tots[0]).astype(BF16), cotb[...], NN)
    wc = width // ns
    for k in range(ns):
        gos[k] = go[:, k * wc:(k + 1) * wc].astype(BF16)
    for dy in (2, 1, 3, 0):
        for dx in (2, 1, 3, 0):
            if dy < ny and dx < nx and (dy or dx):
                py, px = lax.rem(y + dy, ny), lax.rem(x + dx, nx)
                send(gos.at[py * nx + px], gor.at[s_me], go_s, go_r, {"y": py, "x": px})
    far = sorted(range(1, nz), key=lambda k: -min(k, nz - k))

    ksum = xown[...]
    for d in range(1, nx):
        wait_bytes(xr.at[d], x_r.at[d])
        ksum = ksum + xr[d].astype(F32)
    kvs[...] = ksum
    for k in range(nz):
        for cc in range(2):
            zk[2 * k + cc] = kvs[pl.ds(2 * rs * k + rs * cc, rs), :].astype(BF16)
    for dz in far:
        pz = lax.rem(z + dz, nz)
        for cc in (c, o):
            send(zk.at[2 * pz + cc], zr.at[t_me], zk_s, zk_r, {"z": pz, "c": cc})
    send(zk.at[2 * z + o], zr.at[t_me], zk_s, zk_r, {"c": o})
    zr[t_me] = zk[t_me]
    gor[s_me] = gos[s_me]

    l_swin.wait()
    row_at = lax.broadcasted_iota(jnp.int32, (rs, win), 0) + (rs * t_me - w0)
    pick = (lax.broadcasted_iota(jnp.int32, (rs, win), 1) == row_at).astype(F32).astype(BF16)
    sw = dot(pick, swin[...], NN)
    l_twin.wait()
    own_piece = mem == lax.div(z, per)

    @pl.when(own_piece)
    def _():
        wait_bytes(tr.at[pl.ds(0, nz // 2 - 1)], t_r)
        wait_bytes(ts.at[pl.ds(0, pieces - 1)], t_s)

    @pl.when(jnp.logical_not(own_piece))
    def _():
        wait_bytes(tr, t_r)
        wait_bytes(ts, t_s)

    up = jnp.sum(tr[...].astype(F32), axis=0)
    tw = twin[...].astype(F32)
    tw = jnp.where(c == 0, tw[0:rt, :], tw[rt:2 * rt, :])
    gt_o[...] = norm_back(tw, tgb[...], up)

    wait_bytes(gor.at[pl.ds(0, ns - 1)], go_r)
    go_o[...] = jnp.sum(gor[...].astype(F32), axis=0).astype(BF16)

    wait_bytes(zr.at[pl.ds(0, 2 * nz - 1)], zk_r)
    both = [zr[0].astype(F32), zr[1].astype(F32)]
    for k in range(2, 2 * nz):
        both[k % 2] = both[k % 2] + zr[k].astype(F32)
    both = jnp.concatenate(both, axis=1).astype(BF16)
    gs_o[...] = norm_back(sw, sgb[...], dot(both, wkv[...], NT))

    for d in sends:
        d.wait_send()
    wait_bytes(gos.at[pl.ds(0, ns - 1)], go_s)
    wait_bytes(gqo.at[pl.ds(0, 4 * ny - 1)], gq_s)
    wait_bytes(zk.at[pl.ds(0, 2 * nz - 1)], zk_s)


def write_out(a, b, c, a_o, b_o, c_o, sems):
    copies = [pltpu.make_async_copy(i, j, sems.at[k]) for k, (i, j) in enumerate(((a, a_o), (b, b_o), (c, c_o)))]
    for one in copies:
        one.start()
    for one in copies:
        one.wait()


def on_device(shape, target, source, cotangent, target_gain, source_gain, w_query, w_key, w_value, w_out):
    ny, nx, nz = shape
    rows, width = target.shape
    srows = source.shape[0]
    half = srows // 2
    rt, rs = rows // (2 * nz), srows // (2 * nz)
    win = rs if rs % 8 == 0 else rs + 4
    ns = ny * nx
    wide = ny * rows
    vm = pltpu.VMEM
    sem = pltpu.SemaphoreType.DMA
    scratch = [
        vm((half, width), BF16), vm((win, width), BF16), vm((half, width), BF16),
        vm((rows, width), BF16), vm((2 * rt, width), BF16), vm((rows, width), BF16),
        vm((rows, width), BF16), vm((1, width), F32), vm((1, width), F32),
        vm((width, 2 * HEAD), BF16), vm((HEAD, width), BF16),
        vm((nx, 2, half, 2 * HEAD), BF16), vm((ny, rows, 2 * HEAD), BF16),
        vm((nx, 2, half, wide), F32), vm((nx, 2, half, wide), F32),
        vm((nx, 2, half, wide), BF16), vm((nx, 2, half, wide), BF16),
        vm((ny, ny, 2, rows), F32), vm((2 * HEAD, wide), F32), vm((HEAD, wide), F32),
        vm((ny, HEAD, rows), BF16), vm((ny, HEAD, rows), BF16),
        vm((2, nx, srows, HEAD), F32), vm((nx, srows, HEAD), BF16), vm((nx, srows, HEAD), BF16),
        vm((nx, srows, HEAD), BF16), vm((nx, srows, HEAD), BF16), vm((srows, HEAD), F32),
        vm((srows, HEAD), F32), vm((2 * nz, rs, HEAD), BF16), vm((2 * nz, rs, HEAD), BF16),
        vm((4, width, HEAD), BF16), vm((4 * ny, rows // 4, HEAD), BF16), vm((4 * ny, rows // 4, HEAD), BF16),
        vm((rows // 4, width), F32), vm((rows // 4 // rt, rt, width), BF16), vm((nz // 2, rt, width), BF16),
        vm((ns, HEAD, width // ns), BF16), vm((ns, HEAD, width // ns), BF16),
        sem((11,)), sem((nx,)), sem((nx,)), sem((ny,)), sem((ny,)), sem((ny,)), sem((nx,)), sem((nx,)),
        sem, sem((3,)), sem, sem, sem,
        sem((nx,)), sem((nx,)), sem((ny,)), sem((ny,)), sem((ny,)), sem((nx,)), sem((nx,)),
        sem, sem((3,)), sem, sem, sem,
        pltpu.SemaphoreType.REGULAR, pltpu.SemaphoreType.REGULAR, pltpu.SemaphoreType.REGULAR,
    ]
    any_spec = pl.BlockSpec(memory_space=pltpu.HBM)
    vm_spec = pl.BlockSpec(memory_space=pltpu.VMEM)
    made = pl.pallas_call(
        functools.partial(kernel, (ny, nx, nz, 0, rt, rs, win)),
        out_shape=(
            vm((rt, width), BF16), vm((rs, width), BF16), vm((HEAD, width // ns), BF16),
        ),
        in_specs=[any_spec] * 9,
        out_specs=(vm_spec,) * 3,
        scratch_shapes=scratch,
        compiler_params=pltpu.CompilerParams(
            collective_id=0, has_side_effects=True, vmem_limit_bytes=56 * 1024 * 1024
        ),
    )(*(pltpu.with_memory_space_constraint(a, pltpu.HBM) for a in (
        target, source, cotangent, target_gain.reshape(1, width), source_gain.reshape(1, width),
        w_query, w_key, w_value, w_out,
    )))
    return pl.pallas_call(
        write_out,
        out_shape=tuple(jax.ShapeDtypeStruct(m.shape, m.dtype) for m in made),
        in_specs=[vm_spec] * 3,
        out_specs=(pl.BlockSpec(memory_space=pltpu.HBM),) * 3,
        scratch_shapes=[sem((3,))],
        compiler_params=pltpu.CompilerParams(vmem_limit_bytes=1024 * 1024),
    )(*made)


def solution(mesh, ny=4, nx=4):
    nz = mesh.shape["tp"] // 2
    split = Mesh(mesh.devices.reshape(ny, nx, nz, 2), ("y", "x", "z", "c"))
    sp, tp, every = ("y", "x"), ("z", "c"), ("y", "x", "z", "c")
    in_specs = (P(sp, None), P(sp, None), P(sp, None), P(), P(), P(None, tp), P(), P(), P(tp, None))
    out_specs = (P(every, None), P(every, None), P(tp, sp))
    return jax.shard_map(
        functools.partial(on_device, (ny, nx, nz)),
        mesh=split, in_specs=in_specs, out_specs=out_specs, check_vma=False,
    )
```

time: 64 us -> 52.6 us (0.82)
  Pallas kernels: 58.9 us -> 51.9 us
  local copies, waits for them, and re-layouts: 4.18 us -> 0 us
    pallas_call x1, Pallas kernels: 58.9 us -> 51.2 us  [on_device(): pl.pallas_call(functools.partial(kernel, (ny, nx, nz, 0, rt, rs, win)), o...]
    unnamed x3 -> x0, local copies, waits for them, and re-layouts: 4.18 us -> none
    pallas_call x0 -> x1, Pallas kernels: none -> 0.67 us  [on_device(): pl.pallas_call(write_out, out_shape=tuple((jax.ShapeDtypeStruct(m.shape,...]
where the time goes in v2:
time: 52.6 us; the launch traced here: 52.5 us
  Pallas kernels  51.9 us (99%)
  between operations  0.64 us (1%)
    pallas_call x1, Pallas kernels, on_device(): pl.pallas_call(functools.partial(kernel, (ny, nx, nz, 0, rt, rs, win)), o...  51.2 us

profile of v2, /device:TPU:1, one launch (start us, length us, event | category | flops | bytes accessed | tf_op | source)
XLA Modules:
  0.0 52.5 jit_solution(12783335777497328488)
XLA Ops:
  0.6 51.2 %shard_map.112 = (bf16[4,2048]{1,0:T(4,128)(2,1)S(1)}, bf16[12,2048]{1,0:T(8,128)(2,1)S(1)}, bf16[128,128]{1,0:T(8,128)(2,1)S(1)}) custom-call(bf16[128,2048]{1,0:T(8,128)(2,1)} %tgt_h.1, bf16[384,2048]{1,0:T(8,128)(2,1)} %src_h.1, bf16[128,2048]{1,0:T(8,128)(2,1)} %cot_h.1, f32[1,2048]{1,0:T(1,128)} %bitcast.2, f32[1,2048]{1,0:T(1,128)} %bitcast.3, ...), custom_call_target="tpu_custom_call" | custom-call | tf_op jit(solution)/shard_map/pallas_call | solution.py:403
  51.8 0.7 %shard_map.113 = (bf16[4,2048]{1,0:T(4,128)(2,1)}, bf16[12,2048]{1,0:T(8,128)(2,1)}, bf16[128,128]{1,0:T(8,128)(2,1)}) custom-call(bf16[4,2048]{1,0:T(4,128)(2,1)S(1)} %get-tuple-element.6.a, bf16[12,2048]{1,0:T(8,128)(2,1)S(1)} %get-tuple-element.7.b, bf16[128,128]{1,0:T(8,128)(2,1)S(1)} %get-tuple-element.8.c), custom_call_target="tpu_custom_call" | custom-call | tf_op jit(solution)/shard_map/pallas_call | solution.py:418

commit v3 on v2

--- a/solution.py
+++ b/solution.py
@@ -53,7 +53,7 @@
     gt_o, gs_o, go_o,
     srcb, swin, sn, tgtb, twin, tn, cotb, tgb, sgb, wkv, wob,
     kv, qg, est, pgt, e_b, t_b, stat, aw, tk,
-    ys, yr, gkv, ps, pr, xs, xr, xown, kvs, zk, zr,
+    ys, yr, gkv, ps, pr, xs, xr, xown, zk, zr,
     wq4, gqo, gqi, pmat, ts, tr, gos, gor,
     ld, kv_r, kvp_r, qg_r, st_r, y_r, ps_r, x_r, zk_r, wq_r, gq_r, t_r, go_r,
     kv_s, kvp_s, qg_s, st_s, y_s, ps_s, x_s, zk_s, wq_s, gq_s, t_s, go_s,
@@ -66,7 +66,8 @@
     s_me = y * nx + x
     zo = z + 1 - 2 * lax.rem(z, 2)
     zf = lax.rem(z - 1 + 2 * lax.rem(z, 2) + nz, nz)
-    mem = 2 * lax.rem(z, 2) + c
+    hz = lax.rem(z, 2)
+    mem = 2 * hz + c
     half = kv.shape[2]
     rows = tgtb.shape[0]
     width = tgtb.shape[1]
@@ -89,6 +90,8 @@
         peers.extend([{"y": py, "z": zo, "c": c}, {"y": py, "z": zo, "c": o}])
         if dy:
             peers.append({"y": py, "c": o})
+    for dx in range(1, nx):
+        peers.append({"x": lax.rem(x + dx, nx), "z": zo})
     if nz > 2:
         peers.extend([{"z": zf, "c": c}, {"z": zf, "c": o}])
     for peer in peers:
@@ -129,6 +132,12 @@
     l_cot.wait()
     l_wo.wait()
     qg[0, :, pl.ds(HEAD, HEAD)] = dot(cotb[...], wob[...], NT).astype(BF16)
+    l_src.wait()
+    l_sg.wait()
+    norm_rows(srcb, sn, sgb)
+    l_wk.wait()
+    l_wv.wait()
+    kv[0, c] = dot(sn[...], wkv[...], NN).astype(BF16)
     pl.semaphore_wait(barrier, len(peers))
     sends = []
     x_order = [d for d in (2, 1, 3) if d < nx]
@@ -139,13 +148,6 @@
         signal(up_1, {"z": pz})
     sends.append(send(wq4.at[mem], wq4.at[mem], wq_s.at[0], wq_r.at[0], {"z": zo}))
     sends.append(send(wq4.at[mem], wq4.at[mem], wq_s.at[1], wq_r.at[1], {"c": o}))
-
-    l_src.wait()
-    l_sg.wait()
-    norm_rows(srcb, sn, sgb)
-    l_wk.wait()
-    l_wv.wait()
-    kv[0, c] = dot(sn[...], wkv[...], NN).astype(BF16)
     for d in x_order:
         sends.append(send(kv.at[0, c], kv.at[d, c], kv_s.at[d], kv_r.at[d], {"x": lax.rem(x + d, nx)}))
     sends.append(send(kv.at[0, c], kv.at[0, c], kvp_s.at[0], kvp_r.at[0], {"c": o}))
@@ -182,17 +184,13 @@
 
     x_seen = [d for d in (1, 3, 2) if d < nx]
     tot, tilt = unit(0, c, tot, tilt)
-    unit_sums(0, c, True)
     before = 0
     for d in x_seen:
         wait_bytes(kv.at[d, c], kv_r.at[d])
         sends.append(send(kv.at[d, c], kv.at[d, c], kvp_s.at[d], kvp_r.at[d], {"c": o}))
         wait_bytes(kv.at[before, o], kvp_r.at[before])
         tot, tilt = unit(before, o, tot, tilt)
-        unit_sums(before, o, False)
         tot, tilt = unit(d, c, tot, tilt)
-        if d != x_seen[-1]:
-            unit_sums(d, c, False)
         before = d
     wait_bytes(kv.at[before, o], kvp_r.at[before])
     tot, tilt = unit(before, o, tot, tilt)
@@ -202,8 +200,9 @@
         stat[0, e, 1:2, :] = tilt[:, e * rows:(e + 1) * rows]
     for d in y_order:
         sends.append(send(stat.at[0], stat.at[d], st_s.at[d], st_r.at[d], {"y": lax.rem(y + d, ny)}))
-    unit_sums(before, c, False)
-    unit_sums(before, o, False)
+    for d in range(nx):
+        for h in range(2):
+            unit_sums(d, h, d + h == 0)
     for e in y_order:
         ys[e] = aw[pl.ds(HEAD, HEAD), pl.ds(e * rows, rows)].astype(BF16)
         sends.append(send(ys.at[e], yr.at[e], y_s.at[e], y_r.at[e], {"y": lax.rem(y + ny - e, ny)}))
@@ -237,7 +236,21 @@
     q_div = (q_all.astype(F32) * scale).astype(BF16)
     g_div = (g_all.astype(F32) * scale).astype(BF16)
     order = [d for d in (2, 1, 3, 0) if d < nx]
-    for d in order:
+
+    def pass_on(d):
+        wait_bytes(pr.at[d], ps_r.at[d])
+        mine = gkv[c, d] + pr[d].astype(F32)
+        mine = mine.reshape(nz // 2, 2, 2 * rs, HEAD)
+        px = lax.rem(x + nx - d, nx)
+        for h in range(2):
+            if d == 0:
+                xown[h] = mine[:, h]
+            xs[d, h] = mine[:, h].astype(BF16)
+        sends.append(send(xs.at[d, 1 - hz], xr.at[d, 1], x_s.at[d, 1], x_r.at[d, 1], {"x": px, "z": zo}))
+        if d:
+            sends.append(send(xs.at[d, hz], xr.at[d, 0], x_s.at[d, 0], x_r.at[d, 0], {"x": px}))
+
+    for i, d in enumerate(order):
         for h in range(2):
             at = pl.ds(h * half, half)
             dsv = (est[d, h] * (pgt[d, h] - delta)).astype(BF16)
@@ -245,15 +258,10 @@
             gkv[1, d, at, :] = dot(e_b[d, h], g_div, NN)
         ps[d] = gkv[o, d].astype(BF16)
         sends.append(send(ps.at[d], pr.at[d], ps_s.at[d], ps_r.at[d], {"c": o}))
-    for d in order:
-        wait_bytes(pr.at[d], ps_r.at[d])
-        mine = gkv[c, d] + pr[d].astype(F32)
-        if d:
-            xs[d] = mine.astype(BF16)
-            sends.append(send(xs.at[d], xr.at[d], x_s.at[d], x_r.at[d], {"x": lax.rem(x + nx - d, nx)}))
-        else:
-            xown[...] = mine
-
+        if i >= 2:
+            pass_on(order[i - 2])
+    for d in order[-2:] if nx > 1 else order:
+        pass_on(d)
     wait_bytes(wq4.at[0], wq_r.at[0])
     mem_z = 2 * lax.rem(zo, 2) + c
     sends.append(send(wq4.at[mem_z], wq4.at[mem_z], wq_s.at[2], wq_r.at[2], {"c": o}))
@@ -286,6 +294,25 @@
         def _():
             tr[pair] = ts[k]
 
+    far = sorted(range(1, nz), key=lambda k: -min(k, nz - k))
+
+    ksum = xown[hz]
+    for d in range(nx):
+        for h in range(2):
+            if d or h:
+                wait_bytes(xr.at[d, h], x_r.at[d, h])
+                ksum = ksum + xr[d, h].astype(F32)
+    for k in range(nz // 2):
+        for cc in range(2):
+            zk[2 * k + cc] = ksum[k, rs * cc:rs * cc + rs, :].astype(BF16)
+    slot = 2 * lax.div(z, 2) + c
+    for dz in sorted(range(0, nz, 2), key=lambda k: -min(k, nz - k)):
+        pz = lax.rem(z + dz, nz)
+        for cc in (c, o):
+            if dz or cc is o:
+                send(zk.at[2 * lax.div(pz, 2) + cc], zr.at[slot], zk_s, zk_r, {"z": pz, "c": cc})
+    zr[slot] = zk[slot]
+
     for e in range(1, ny):
         wait_bytes(yr.at[e], y_r.at[e])
     av = aw[pl.ds(HEAD, HEAD), pl.ds(0, rows)]
@@ -300,22 +327,6 @@
             if dy < ny and dx < nx and (dy or dx):
                 py, px = lax.rem(y + dy, ny), lax.rem(x + dx, nx)
                 send(gos.at[py * nx + px], gor.at[s_me], go_s, go_r, {"y": py, "x": px})
-    far = sorted(range(1, nz), key=lambda k: -min(k, nz - k))
-
-    ksum = xown[...]
-    for d in range(1, nx):
-        wait_bytes(xr.at[d], x_r.at[d])
-        ksum = ksum + xr[d].astype(F32)
-    kvs[...] = ksum
-    for k in range(nz):
-        for cc in range(2):
-            zk[2 * k + cc] = kvs[pl.ds(2 * rs * k + rs * cc, rs), :].astype(BF16)
-    for dz in far:
-        pz = lax.rem(z + dz, nz)
-        for cc in (c, o):
-            send(zk.at[2 * pz + cc], zr.at[t_me], zk_s, zk_r, {"z": pz, "c": cc})
-    send(zk.at[2 * z + o], zr.at[t_me], zk_s, zk_r, {"c": o})
-    zr[t_me] = zk[t_me]
     gor[s_me] = gos[s_me]
 
     l_swin.wait()
@@ -343,9 +354,9 @@
     wait_bytes(gor.at[pl.ds(0, ns - 1)], go_r)
     go_o[...] = jnp.sum(gor[...].astype(F32), axis=0).astype(BF16)
 
-    wait_bytes(zr.at[pl.ds(0, 2 * nz - 1)], zk_r)
+    wait_bytes(zr.at[pl.ds(0, nz - 1)], zk_r)
     both = [zr[0].astype(F32), zr[1].astype(F32)]
-    for k in range(2, 2 * nz):
+    for k in range(2, nz):
         both[k % 2] = both[k % 2] + zr[k].astype(F32)
     both = jnp.concatenate(both, axis=1).astype(BF16)
     gs_o[...] = norm_back(sw, sgb[...], dot(both, wkv[...], NT))
@@ -354,7 +365,7 @@
         d.wait_send()
     wait_bytes(gos.at[pl.ds(0, ns - 1)], go_s)
     wait_bytes(gqo.at[pl.ds(0, 4 * ny - 1)], gq_s)
-    wait_bytes(zk.at[pl.ds(0, 2 * nz - 1)], zk_s)
+    wait_bytes(zk.at[pl.ds(0, nz - 1)], zk_s)
 
 
 def write_out(a, b, c, a_o, b_o, c_o, sems):
@@ -387,14 +398,14 @@
         vm((ny, ny, 2, rows), F32), vm((2 * HEAD, wide), F32), vm((HEAD, wide), F32),
         vm((ny, HEAD, rows), BF16), vm((ny, HEAD, rows), BF16),
         vm((2, nx, srows, HEAD), F32), vm((nx, srows, HEAD), BF16), vm((nx, srows, HEAD), BF16),
-        vm((nx, srows, HEAD), BF16), vm((nx, srows, HEAD), BF16), vm((srows, HEAD), F32),
-        vm((srows, HEAD), F32), vm((2 * nz, rs, HEAD), BF16), vm((2 * nz, rs, HEAD), BF16),
+        vm((nx, 2, nz // 2, 2 * rs, HEAD), BF16), vm((nx, 2, nz // 2, 2 * rs, HEAD), BF16),
+        vm((2, nz // 2, 2 * rs, HEAD), F32), vm((nz, rs, HEAD), BF16), vm((nz, rs, HEAD), BF16),
         vm((4, width, HEAD), BF16), vm((4 * ny, rows // 4, HEAD), BF16), vm((4 * ny, rows // 4, HEAD), BF16),
         vm((rows // 4, width), F32), vm((rows // 4 // rt, rt, width), BF16), vm((nz // 2, rt, width), BF16),
         vm((ns, HEAD, width // ns), BF16), vm((ns, HEAD, width // ns), BF16),
-        sem((11,)), sem((nx,)), sem((nx,)), sem((ny,)), sem((ny,)), sem((ny,)), sem((nx,)), sem((nx,)),
+        sem((11,)), sem((nx,)), sem((nx,)), sem((ny,)), sem((ny,)), sem((ny,)), sem((nx,)), sem((nx, 2)),
         sem, sem((3,)), sem, sem, sem,
-        sem((nx,)), sem((nx,)), sem((ny,)), sem((ny,)), sem((ny,)), sem((nx,)), sem((nx,)),
+        sem((nx,)), sem((nx,)), sem((ny,)), sem((ny,)), sem((ny,)), sem((nx,)), sem((nx, 2)),
         sem, sem((3,)), sem, sem, sem,
         pltpu.SemaphoreType.REGULAR, pltpu.SemaphoreType.REGULAR, pltpu.SemaphoreType.REGULAR,
     ]

time: 52.6 us -> 51.4 us (0.977)
  Pallas kernels: 51.9 us -> 50.7 us
    pallas_call x1, Pallas kernels: 51.2 us -> 50 us  [on_device(): pl.pallas_call(functools.partial(kernel, (ny, nx, nz, 0, rt, rs, win)), o...]
where the time goes in v3:
time: 51.4 us; the launch traced here: 51.3 us
  Pallas kernels  50.7 us (99%)
  between operations  0.64 us (1%)
    pallas_call x1, Pallas kernels, on_device(): pl.pallas_call(functools.partial(kernel, (ny, nx, nz, 0, rt, rs, win)), o...  50 us

profile of v3, /device:TPU:1, one launch (start us, length us, event | category | flops | bytes accessed | tf_op | source)
XLA Modules:
  0.0 51.3 jit_solution(16009838426832874606)
XLA Ops:
  0.6 50.0 %shard_map.112 = (bf16[4,2048]{1,0:T(4,128)(2,1)S(1)}, bf16[12,2048]{1,0:T(8,128)(2,1)S(1)}, bf16[128,128]{1,0:T(8,128)(2,1)S(1)}) custom-call(bf16[128,2048]{1,0:T(8,128)(2,1)} %tgt_h.1, bf16[384,2048]{1,0:T(8,128)(2,1)} %src_h.1, bf16[128,2048]{1,0:T(8,128)(2,1)} %cot_h.1, f32[1,2048]{1,0:T(1,128)} %bitcast.2, f32[1,2048]{1,0:T(1,128)} %bitcast.3, ...), custom_call_target="tpu_custom_call" | custom-call | tf_op jit(solution)/shard_map/pallas_call | solution.py:414
  50.6 0.7 %shard_map.113 = (bf16[4,2048]{1,0:T(4,128)(2,1)}, bf16[12,2048]{1,0:T(8,128)(2,1)}, bf16[128,128]{1,0:T(8,128)(2,1)}) custom-call(bf16[4,2048]{1,0:T(4,128)(2,1)S(1)} %get-tuple-element.6.a, bf16[12,2048]{1,0:T(8,128)(2,1)S(1)} %get-tuple-element.7.b, bf16[128,128]{1,0:T(8,128)(2,1)S(1)} %get-tuple-element.8.c), custom_call_target="tpu_custom_call" | custom-call | tf_op jit(solution)/shard_map/pallas_call | solution.py:429

commit v4 on v3

--- a/solution.py
+++ b/solution.py
@@ -57,7 +57,7 @@
     wq4, gqo, gqi, pmat, ts, tr, gos, gor,
     ld, kv_r, kvp_r, qg_r, st_r, y_r, ps_r, x_r, zk_r, wq_r, gq_r, t_r, go_r,
     kv_s, kvp_s, qg_s, st_s, y_s, ps_s, x_s, zk_s, wq_s, gq_s, t_s, go_s,
-    up_1, up_2, up_4,
+    up_1, up_2, up_4, seen_x, seen_y,
 ):
     ny, nx, nz, gsz, rt, rs, win = dims
     ns = ny * nx
@@ -68,6 +68,7 @@
     zf = lax.rem(z - 1 + 2 * lax.rem(z, 2) + nz, nz)
     hz = lax.rem(z, 2)
     mem = 2 * hz + c
+    zp = lax.select(c == 0, zo, zf)
     half = kv.shape[2]
     rows = tgtb.shape[0]
     width = tgtb.shape[1]
@@ -81,19 +82,11 @@
         return [lax.rem(z + k, nz), lax.rem(z + nz - k, nz)] if 2 * k < nz else [lax.rem(z + k, nz)]
 
     peers = [{"c": o}]
-    for dy in range(ny):
-        for dx in range(nx):
-            if dy or dx:
-                peers.append({"y": lax.rem(y + dy, ny), "x": lax.rem(x + dx, nx)})
-    for dy in range(ny):
-        py = lax.rem(y + dy, ny)
-        peers.extend([{"y": py, "z": zo, "c": c}, {"y": py, "z": zo, "c": o}])
-        if dy:
-            peers.append({"y": py, "c": o})
-    for dx in range(1, nx):
-        peers.append({"x": lax.rem(x + dx, nx), "z": zo})
-    if nz > 2:
-        peers.extend([{"z": zf, "c": c}, {"z": zf, "c": o}])
+    x_peers = [{"x": lax.rem(x + dx, nx)} for dx in range(1, nx)]
+    y_peers = [{"y": lax.rem(y + dy, ny)} for dy in range(1, ny)]
+    peers.extend(x_peers + y_peers)
+    for pz in [zo, zf] if nz > 2 else [zo]:
+        peers.extend([{"z": pz, "c": c}, {"z": pz, "c": o}])
     for peer in peers:
         signal(barrier, peer)
 
@@ -132,22 +125,26 @@
     l_cot.wait()
     l_wo.wait()
     qg[0, :, pl.ds(HEAD, HEAD)] = dot(cotb[...], wob[...], NT).astype(BF16)
+    pl.semaphore_wait(barrier, len(peers))
+    sends = []
+    x_order = [d for d in (2, 1, 3) if d < nx]
+    y_order = [d for d in (2, 1, 3) if d < ny]
+    for d in y_order:
+        sends.append(send(qg.at[0], qg.at[d], qg_s.at[d], qg_r.at[d], {"y": lax.rem(y + d, ny)}))
+    for peer in y_peers:
+        signal(seen_y, peer)
+    for peer in x_peers:
+        signal(seen_x, peer)
+    for pz in beside(1):
+        signal(up_1, {"z": pz})
+    sends.append(send(wq4.at[mem], wq4.at[mem], wq_s.at[0], wq_r.at[0], {"z": zo}))
+    sends.append(send(wq4.at[mem], wq4.at[mem], wq_s.at[1], wq_r.at[1], {"c": o}))
     l_src.wait()
     l_sg.wait()
     norm_rows(srcb, sn, sgb)
     l_wk.wait()
     l_wv.wait()
     kv[0, c] = dot(sn[...], wkv[...], NN).astype(BF16)
-    pl.semaphore_wait(barrier, len(peers))
-    sends = []
-    x_order = [d for d in (2, 1, 3) if d < nx]
-    y_order = [d for d in (2, 1, 3) if d < ny]
-    for d in y_order:
-        sends.append(send(qg.at[0], qg.at[d], qg_s.at[d], qg_r.at[d], {"y": lax.rem(y + d, ny)}))
-    for pz in beside(1):
-        signal(up_1, {"z": pz})
-    sends.append(send(wq4.at[mem], wq4.at[mem], wq_s.at[0], wq_r.at[0], {"z": zo}))
-    sends.append(send(wq4.at[mem], wq4.at[mem], wq_s.at[1], wq_r.at[1], {"c": o}))
     for d in x_order:
         sends.append(send(kv.at[0, c], kv.at[d, c], kv_s.at[d], kv_r.at[d], {"x": lax.rem(x + d, nx)}))
     sends.append(send(kv.at[0, c], kv.at[0, c], kvp_s.at[0], kvp_r.at[0], {"c": o}))
@@ -218,6 +215,7 @@
     inv_total = jnp.concatenate(tots, axis=1)
     delta = jnp.concatenate(deltas, axis=1)
 
+    pl.semaphore_wait(seen_y, len(y_peers))
     gq = ((tk[...] - delta * aw[pl.ds(0, HEAD), :]) * (inv_total * INV_ROOT)).T.astype(BF16)
     quarter = rows // 4
     for e in range(ny):
@@ -232,6 +230,7 @@
                 to = 2 * lax.rem(pz, 2) + pc
                 send(gqo.at[4 * e + to], gqi.at[4 * e + mem], gq_s, gq_r, {"y": py, "z": pz, "c": pc})
     gqi[mem] = gqo[mem]
+    pl.semaphore_wait(seen_x, len(x_peers))
     scale = jnp.broadcast_to(inv_total, (8, ny * rows)).T[:, 0:1]
     q_div = (q_all.astype(F32) * scale).astype(BF16)
     g_div = (g_all.astype(F32) * scale).astype(BF16)
@@ -246,7 +245,7 @@
             if d == 0:
                 xown[h] = mine[:, h]
             xs[d, h] = mine[:, h].astype(BF16)
-        sends.append(send(xs.at[d, 1 - hz], xr.at[d, 1], x_s.at[d, 1], x_r.at[d, 1], {"x": px, "z": zo}))
+        sends.append(send(xs.at[d, 1 - hz], xr.at[d, 1], x_s.at[d, 1], x_r.at[d, 1], {"x": px, "z": zp}))
         if d:
             sends.append(send(xs.at[d, hz], xr.at[d, 0], x_s.at[d, 0], x_r.at[d, 0], {"x": px}))
 
@@ -408,6 +407,7 @@
         sem((nx,)), sem((nx,)), sem((ny,)), sem((ny,)), sem((ny,)), sem((nx,)), sem((nx, 2)),
         sem, sem((3,)), sem, sem, sem,
         pltpu.SemaphoreType.REGULAR, pltpu.SemaphoreType.REGULAR, pltpu.SemaphoreType.REGULAR,
+        pltpu.SemaphoreType.REGULAR, pltpu.SemaphoreType.REGULAR,
     ]
     any_spec = pl.BlockSpec(memory_space=pltpu.HBM)
     vm_spec = pl.BlockSpec(memory_space=pltpu.VMEM)

time: 51.4 us -> 48.8 us (0.949)
  Pallas kernels: 50.7 us -> 48.1 us
    pallas_call x1, Pallas kernels: 50 us -> 47.4 us  [on_device(): pl.pallas_call(functools.partial(kernel, (ny, nx, nz, 0, rt, rs, win)), o...]
where the time goes in v4:
time: 48.8 us; the launch traced here: 48.7 us
  Pallas kernels  48.1 us (99%)
  between operations  0.64 us (1%)
    pallas_call x1, Pallas kernels, on_device(): pl.pallas_call(functools.partial(kernel, (ny, nx, nz, 0, rt, rs, win)), o...  47.4 us

profile of v4, /device:TPU:1, one launch (start us, length us, event | category | flops | bytes accessed | tf_op | source)
XLA Modules:
  0.0 48.7 jit_solution(9289685013966770685)
XLA Ops:
  0.6 47.4 %shard_map.112 = (bf16[4,2048]{1,0:T(4,128)(2,1)S(1)}, bf16[12,2048]{1,0:T(8,128)(2,1)S(1)}, bf16[128,128]{1,0:T(8,128)(2,1)S(1)}) custom-call(bf16[128,2048]{1,0:T(8,128)(2,1)} %tgt_h.1, bf16[384,2048]{1,0:T(8,128)(2,1)} %src_h.1, bf16[128,2048]{1,0:T(8,128)(2,1)} %cot_h.1, f32[1,2048]{1,0:T(1,128)} %bitcast.2, f32[1,2048]{1,0:T(1,128)} %bitcast.3, ...), custom_call_target="tpu_custom_call" | custom-call | tf_op jit(solution)/shard_map/pallas_call | solution.py:414
  48.1 0.7 %shard_map.113 = (bf16[4,2048]{1,0:T(4,128)(2,1)}, bf16[12,2048]{1,0:T(8,128)(2,1)}, bf16[128,128]{1,0:T(8,128)(2,1)}) custom-call(bf16[4,2048]{1,0:T(4,128)(2,1)S(1)} %get-tuple-element.6.a, bf16[12,2048]{1,0:T(8,128)(2,1)S(1)} %get-tuple-element.7.b, bf16[128,128]{1,0:T(8,128)(2,1)S(1)} %get-tuple-element.8.c), custom_call_target="tpu_custom_call" | custom-call | tf_op jit(solution)/shard_map/pallas_call | solution.py:429

commit v5 on v4

--- a/solution.py
+++ b/solution.py
@@ -52,7 +52,7 @@
     dims, tgt_h, src_h, cot_h, tg_h, sg_h, wq_h, wk_h, wv_h, wo_h,
     gt_o, gs_o, go_o,
     srcb, swin, sn, tgtb, twin, tn, cotb, tgb, sgb, wkv, wob,
-    kv, qg, est, pgt, e_b, t_b, stat, aw, tk,
+    kv, qg, est, pgt, lhs, t_b, rhs, stat, aw, tk,
     ys, yr, gkv, ps, pr, xs, xr, xown, zk, zr,
     wq4, gqo, gqi, pmat, ts, tr, gos, gor,
     ld, kv_r, kvp_r, qg_r, st_r, y_r, ps_r, x_r, zk_r, wq_r, gq_r, t_r, go_r,
@@ -127,7 +127,7 @@
     qg[0, :, pl.ds(HEAD, HEAD)] = dot(cotb[...], wob[...], NT).astype(BF16)
     pl.semaphore_wait(barrier, len(peers))
     sends = []
-    x_order = [d for d in (2, 1, 3) if d < nx]
+    x_order = [d for d in (1, 3, 2) if d < nx]
     y_order = [d for d in (2, 1, 3) if d < ny]
     for d in y_order:
         sends.append(send(qg.at[0], qg.at[d], qg_s.at[d], qg_r.at[d], {"y": lax.rem(y + d, ny)}))
@@ -169,12 +169,12 @@
         t = e * g
         est[d, h] = e
         pgt[d, h] = g
-        e_b[d, h] = e.astype(BF16)
+        lhs[1, d, h] = e.astype(BF16)
         t_b[d, h] = t.astype(BF16)
         return tot + jnp.sum(e, axis=0, keepdims=True), tilt + jnp.sum(t, axis=0, keepdims=True)
 
     def unit_sums(d, h, first):
-        both = dot(kv[d, h], e_b[d, h], TN)
+        both = dot(kv[d, h], lhs[1, d, h], TN)
         one = dot(kv[d, h, :, pl.ds(0, HEAD)], t_b[d, h], TN)
         aw[...] = both if first else aw[...] + both
         tk[...] = one if first else tk[...] + one
@@ -232,13 +232,23 @@
     gqi[mem] = gqo[mem]
     pl.semaphore_wait(seen_x, len(x_peers))
     scale = jnp.broadcast_to(inv_total, (8, ny * rows)).T[:, 0:1]
-    q_div = (q_all.astype(F32) * scale).astype(BF16)
-    g_div = (g_all.astype(F32) * scale).astype(BF16)
+    rhs[0] = (q_all.astype(F32) * (scale * INV_ROOT)).astype(BF16)
+    rhs[1] = (g_all.astype(F32) * scale).astype(BF16)
     order = [d for d in (2, 1, 3, 0) if d < nx]
+
+    def other(d):
+        for h in range(2):
+            lhs[0, d, h] = (est[d, h] * (pgt[d, h] - delta)).astype(BF16)
+            ps[d, pl.ds(h * half, half), :] = dot(lhs[o, d, h], rhs[o], NN).astype(BF16)
+        sends.append(send(ps.at[d], pr.at[d], ps_s.at[d], ps_r.at[d], {"c": o}))
+
+    def own(d):
+        for h in range(2):
+            gkv[d, pl.ds(h * half, half), :] = dot(lhs[c, d, h], rhs[c], NN)
 
     def pass_on(d):
         wait_bytes(pr.at[d], ps_r.at[d])
-        mine = gkv[c, d] + pr[d].astype(F32)
+        mine = gkv[d] + pr[d].astype(F32)
         mine = mine.reshape(nz // 2, 2, 2 * rs, HEAD)
         px = lax.rem(x + nx - d, nx)
         for h in range(2):
@@ -249,21 +259,19 @@
         if d:
             sends.append(send(xs.at[d, hz], xr.at[d, 0], x_s.at[d, 0], x_r.at[d, 0], {"x": px}))
 
-    for i, d in enumerate(order):
-        for h in range(2):
-            at = pl.ds(h * half, half)
-            dsv = (est[d, h] * (pgt[d, h] - delta)).astype(BF16)
-            gkv[0, d, at, :] = dot(dsv, q_div, NN) * INV_ROOT
-            gkv[1, d, at, :] = dot(e_b[d, h], g_div, NN)
-        ps[d] = gkv[o, d].astype(BF16)
-        sends.append(send(ps.at[d], pr.at[d], ps_s.at[d], ps_r.at[d], {"c": o}))
-        if i >= 2:
-            pass_on(order[i - 2])
-    for d in order[-2:] if nx > 1 else order:
-        pass_on(d)
+    steps = [(other, order[0])]
+    for i in range(len(order)):
+        if i + 1 < len(order):
+            steps.append((other, order[i + 1]))
+        steps.append((own, order[i]))
+        if i:
+            steps.append((pass_on, order[i - 1]))
+    for step, d in steps:
+        step(d)
     wait_bytes(wq4.at[0], wq_r.at[0])
     mem_z = 2 * lax.rem(zo, 2) + c
     sends.append(send(wq4.at[mem_z], wq4.at[mem_z], wq_s.at[2], wq_r.at[2], {"c": o}))
+    pass_on(order[-1])
     wait_bytes(gqi.at[pl.ds(0, 4 * ny - 1)], gq_r)
     wait_bytes(wq4.at[0], wq_r.at[1])
     wait_bytes(wq4.at[0], wq_r.at[2])
@@ -393,10 +401,10 @@
         vm((width, 2 * HEAD), BF16), vm((HEAD, width), BF16),
         vm((nx, 2, half, 2 * HEAD), BF16), vm((ny, rows, 2 * HEAD), BF16),
         vm((nx, 2, half, wide), F32), vm((nx, 2, half, wide), F32),
-        vm((nx, 2, half, wide), BF16), vm((nx, 2, half, wide), BF16),
+        vm((2, nx, 2, half, wide), BF16), vm((nx, 2, half, wide), BF16), vm((2, wide, HEAD), BF16),
         vm((ny, ny, 2, rows), F32), vm((2 * HEAD, wide), F32), vm((HEAD, wide), F32),
         vm((ny, HEAD, rows), BF16), vm((ny, HEAD, rows), BF16),
-        vm((2, nx, srows, HEAD), F32), vm((nx, srows, HEAD), BF16), vm((nx, srows, HEAD), BF16),
+        vm((nx, srows, HEAD), F32), vm((nx, srows, HEAD), BF16), vm((nx, srows, HEAD), BF16),
         vm((nx, 2, nz // 2, 2 * rs, HEAD), BF16), vm((nx, 2, nz // 2, 2 * rs, HEAD), BF16),
         vm((2, nz // 2, 2 * rs, HEAD), F32), vm((nz, rs, HEAD), BF16), vm((nz, rs, HEAD), BF16),
         vm((4, width, HEAD), BF16), vm((4 * ny, rows // 4, HEAD), BF16), vm((4 * ny, rows // 4, HEAD), BF16),

time: 48.8 us -> 47 us (0.963)
  Pallas kernels: 48.1 us -> 46.2 us
    pallas_call x1, Pallas kernels: 47.4 us -> 45.5 us  [on_device(): pl.pallas_call(functools.partial(kernel, (ny, nx, nz, 0, rt, rs, win)), o...]
where the time goes in v5:
time: 47 us; the launch traced here: 46.9 us
  Pallas kernels  46.2 us (98%)
  between operations  0.64 us (1%)
    pallas_call x1, Pallas kernels, on_device(): pl.pallas_call(functools.partial(kernel, (ny, nx, nz, 0, rt, rs, win)), o...  45.5 us

profile of v5, /device:TPU:1, one launch (start us, length us, event | category | flops | bytes accessed | tf_op | source)
XLA Modules:
  0.0 46.9 jit_solution(15894545185334423747)
XLA Ops:
  0.6 45.5 %shard_map.112 = (bf16[4,2048]{1,0:T(4,128)(2,1)S(1)}, bf16[12,2048]{1,0:T(8,128)(2,1)S(1)}, bf16[128,128]{1,0:T(8,128)(2,1)S(1)}) custom-call(bf16[128,2048]{1,0:T(8,128)(2,1)} %tgt_h.1, bf16[384,2048]{1,0:T(8,128)(2,1)} %src_h.1, bf16[128,2048]{1,0:T(8,128)(2,1)} %cot_h.1, f32[1,2048]{1,0:T(1,128)} %bitcast.2, f32[1,2048]{1,0:T(1,128)} %bitcast.3, ...), custom_call_target="tpu_custom_call" | custom-call | tf_op jit(solution)/shard_map/pallas_call | solution.py:422
  46.2 0.7 %shard_map.113 = (bf16[4,2048]{1,0:T(4,128)(2,1)}, bf16[12,2048]{1,0:T(8,128)(2,1)}, bf16[128,128]{1,0:T(8,128)(2,1)}) custom-call(bf16[4,2048]{1,0:T(4,128)(2,1)S(1)} %get-tuple-element.6.a, bf16[12,2048]{1,0:T(8,128)(2,1)S(1)} %get-tuple-element.7.b, bf16[128,128]{1,0:T(8,128)(2,1)S(1)} %get-tuple-element.8.c), custom_call_target="tpu_custom_call" | custom-call | tf_op jit(solution)/shard_map/pallas_call | solution.py:437

commit v6 on v5

--- a/solution.py
+++ b/solution.py
@@ -266,11 +266,13 @@
         steps.append((own, order[i]))
         if i:
             steps.append((pass_on, order[i - 1]))
-    for step, d in steps:
+    for step, d in steps[:5]:
         step(d)
     wait_bytes(wq4.at[0], wq_r.at[0])
     mem_z = 2 * lax.rem(zo, 2) + c
     sends.append(send(wq4.at[mem_z], wq4.at[mem_z], wq_s.at[2], wq_r.at[2], {"c": o}))
+    for step, d in steps[5:]:
+        step(d)
     pass_on(order[-1])
     wait_bytes(gqi.at[pl.ds(0, 4 * ny - 1)], gq_r)
     wait_bytes(wq4.at[0], wq_r.at[1])
@@ -311,7 +313,7 @@
                 ksum = ksum + xr[d, h].astype(F32)
     for k in range(nz // 2):
         for cc in range(2):
-            zk[2 * k + cc] = ksum[k, rs * cc:rs * cc + rs, :].astype(BF16)
+            zk[2 * k + cc] = ksum[k, rs * cc:rs * cc + rs, :].reshape(rs // 4, 4, HEAD).astype(BF16)
     slot = 2 * lax.div(z, 2) + c
     for dz in sorted(range(0, nz, 2), key=lambda k: -min(k, nz - k)):
         pz = lax.rem(z + dz, nz)
@@ -365,7 +367,7 @@
     both = [zr[0].astype(F32), zr[1].astype(F32)]
     for k in range(2, nz):
         both[k % 2] = both[k % 2] + zr[k].astype(F32)
-    both = jnp.concatenate(both, axis=1).astype(BF16)
+    both = jnp.concatenate([one.reshape(rs, HEAD) for one in both], axis=1).astype(BF16)
     gs_o[...] = norm_back(sw, sgb[...], dot(both, wkv[...], NT))
 
     for d in sends:
@@ -406,7 +408,7 @@
         vm((ny, HEAD, rows), BF16), vm((ny, HEAD, rows), BF16),
         vm((nx, srows, HEAD), F32), vm((nx, srows, HEAD), BF16), vm((nx, srows, HEAD), BF16),
         vm((nx, 2, nz // 2, 2 * rs, HEAD), BF16), vm((nx, 2, nz // 2, 2 * rs, HEAD), BF16),
-        vm((2, nz // 2, 2 * rs, HEAD), F32), vm((nz, rs, HEAD), BF16), vm((nz, rs, HEAD), BF16),
+        vm((2, nz // 2, 2 * rs, HEAD), F32), vm((nz, rs // 4, 4, HEAD), BF16), vm((nz, rs // 4, 4, HEAD), BF16),
         vm((4, width, HEAD), BF16), vm((4 * ny, rows // 4, HEAD), BF16), vm((4 * ny, rows // 4, HEAD), BF16),
         vm((rows // 4, width), F32), vm((rows // 4 // rt, rt, width), BF16), vm((nz // 2, rt, width), BF16),
         vm((ns, HEAD, width // ns), BF16), vm((ns, HEAD, width // ns), BF16),

time: 47 us -> 46.3 us (0.985)
  Pallas kernels: 46.2 us -> 45.5 us
    pallas_call x1, Pallas kernels: 45.5 us -> 44.8 us  [on_device(): pl.pallas_call(functools.partial(kernel, (ny, nx, nz, 0, rt, rs, win)), o...]
where the time goes in v6:
time: 46.3 us; the launch traced here: 46.1 us
  Pallas kernels  45.5 us (98%)
  between operations  0.64 us (1%)
    pallas_call x1, Pallas kernels, on_device(): pl.pallas_call(functools.partial(kernel, (ny, nx, nz, 0, rt, rs, win)), o...  44.8 us

profile of v6, /device:TPU:1, one launch (start us, length us, event | category | flops | bytes accessed | tf_op | source)
XLA Modules:
  0.0 46.1 jit_solution(8948399053609313419)
XLA Ops:
  0.6 44.8 %shard_map.112 = (bf16[4,2048]{1,0:T(4,128)(2,1)S(1)}, bf16[12,2048]{1,0:T(8,128)(2,1)S(1)}, bf16[128,128]{1,0:T(8,128)(2,1)S(1)}) custom-call(bf16[128,2048]{1,0:T(8,128)(2,1)} %tgt_h.1, bf16[384,2048]{1,0:T(8,128)(2,1)} %src_h.1, bf16[128,2048]{1,0:T(8,128)(2,1)} %cot_h.1, f32[1,2048]{1,0:T(1,128)} %bitcast.2, f32[1,2048]{1,0:T(1,128)} %bitcast.3, ...), custom_call_target="tpu_custom_call" | custom-call | tf_op jit(solution)/shard_map/pallas_call | solution.py:424
  45.5 0.7 %shard_map.113 = (bf16[4,2048]{1,0:T(4,128)(2,1)}, bf16[12,2048]{1,0:T(8,128)(2,1)}, bf16[128,128]{1,0:T(8,128)(2,1)}) custom-call(bf16[4,2048]{1,0:T(4,128)(2,1)S(1)} %get-tuple-element.6.a, bf16[12,2048]{1,0:T(8,128)(2,1)S(1)} %get-tuple-element.7.b, bf16[128,128]{1,0:T(8,128)(2,1)S(1)} %get-tuple-element.8.c), custom_call_target="tpu_custom_call" | custom-call | tf_op jit(solution)/shard_map/pallas_call | solution.py:439

commit v7 on v6

--- a/solution.py
+++ b/solution.py
@@ -164,7 +164,7 @@
 
     def unit(d, h, tot, tilt):
         key, val = kv[d, h, :, pl.ds(0, HEAD)], kv[d, h, :, pl.ds(HEAD, HEAD)]
-        e = jnp.exp2(dot(key, q_all, NT) * (INV_ROOT * LOG2E))
+        e = jnp.exp2(dot(key, q_all, NT) * (INV_ROOT * LOG2E) - 2.0)
         g = dot(val, g_all, NT)
         t = e * g
         est[d, h] = e
@@ -231,20 +231,23 @@
                 send(gqo.at[4 * e + to], gqi.at[4 * e + mem], gq_s, gq_r, {"y": py, "z": pz, "c": pc})
     gqi[mem] = gqo[mem]
     pl.semaphore_wait(seen_x, len(x_peers))
-    scale = jnp.broadcast_to(inv_total, (8, ny * rows)).T[:, 0:1]
-    rhs[0] = (q_all.astype(F32) * (scale * INV_ROOT)).astype(BF16)
-    rhs[1] = (g_all.astype(F32) * scale).astype(BF16)
+    rhs[0] = q_all
+    rhs[1] = g_all
+    root = lax.select(c == 0, jnp.float32(INV_ROOT), jnp.float32(1.0))
+    root_o = lax.select(c == 0, jnp.float32(1.0), jnp.float32(INV_ROOT))
     order = [d for d in (2, 1, 3, 0) if d < nx]
 
     def other(d):
         for h in range(2):
-            lhs[0, d, h] = (est[d, h] * (pgt[d, h] - delta)).astype(BF16)
-            ps[d, pl.ds(h * half, half), :] = dot(lhs[o, d, h], rhs[o], NN).astype(BF16)
+            p = est[d, h] * inv_total
+            lhs[0, d, h] = (p * (pgt[d, h] - delta)).astype(BF16)
+            lhs[1, d, h] = p.astype(BF16)
+            ps[d, pl.ds(h * half, half), :] = (dot(lhs[o, d, h], rhs[o], NN) * root_o).astype(BF16)
         sends.append(send(ps.at[d], pr.at[d], ps_s.at[d], ps_r.at[d], {"c": o}))
 
     def own(d):
         for h in range(2):
-            gkv[d, pl.ds(h * half, half), :] = dot(lhs[c, d, h], rhs[c], NN)
+            gkv[d, pl.ds(h * half, half), :] = dot(lhs[c, d, h], rhs[c], NN) * root
 
     def pass_on(d):
         wait_bytes(pr.at[d], ps_r.at[d])

time: 46.3 us -> 46 us (level)
  no operation moved by 1% of the time
where the time goes in v7:
time: 46 us; the launch traced here: 45.9 us
  Pallas kernels  45.2 us (98%)
  between operations  0.64 us (1%)
    pallas_call x1, Pallas kernels, on_device(): pl.pallas_call(functools.partial(kernel, (ny, nx, nz, 0, rt, rs, win)), o...  44.6 us

profile of v7, /device:TPU:1, one launch (start us, length us, event | category | flops | bytes accessed | tf_op | source)
XLA Modules:
  0.0 45.9 jit_solution(18217948056224477327)
XLA Ops:
  0.6 44.6 %shard_map.112 = (bf16[4,2048]{1,0:T(4,128)(2,1)S(1)}, bf16[12,2048]{1,0:T(8,128)(2,1)S(1)}, bf16[128,128]{1,0:T(8,128)(2,1)S(1)}) custom-call(bf16[128,2048]{1,0:T(8,128)(2,1)} %tgt_h.1, bf16[384,2048]{1,0:T(8,128)(2,1)} %src_h.1, bf16[128,2048]{1,0:T(8,128)(2,1)} %cot_h.1, f32[1,2048]{1,0:T(1,128)} %bitcast.2, f32[1,2048]{1,0:T(1,128)} %bitcast.3, ...), custom_call_target="tpu_custom_call" | custom-call | tf_op jit(solution)/shard_map/pallas_call | solution.py:427
  45.2 0.7 %shard_map.113 = (bf16[4,2048]{1,0:T(4,128)(2,1)}, bf16[12,2048]{1,0:T(8,128)(2,1)}, bf16[128,128]{1,0:T(8,128)(2,1)}) custom-call(bf16[4,2048]{1,0:T(4,128)(2,1)S(1)} %get-tuple-element.6.a, bf16[12,2048]{1,0:T(8,128)(2,1)S(1)} %get-tuple-element.7.b, bf16[128,128]{1,0:T(8,128)(2,1)S(1)} %get-tuple-element.8.c), custom_call_target="tpu_custom_call" | custom-call | tf_op jit(solution)/shard_map/pallas_call | solution.py:442

commit v8 on v7

--- a/solution.py
+++ b/solution.py
@@ -266,9 +266,9 @@
     for i in range(len(order)):
         if i + 1 < len(order):
             steps.append((other, order[i + 1]))
-        steps.append((own, order[i]))
         if i:
             steps.append((pass_on, order[i - 1]))
+        steps.append((own, order[i]))
     for step, d in steps[:5]:
         step(d)
     wait_bytes(wq4.at[0], wq_r.at[0])

time: 46 us -> 46 us (level)
  no operation moved by 1% of the time
where the time goes in v8:
time: 46 us; the launch traced here: 45.9 us
  Pallas kernels  45.2 us (98%)
  between operations  0.64 us (1%)
    pallas_call x1, Pallas kernels, on_device(): pl.pallas_call(functools.partial(kernel, (ny, nx, nz, 0, rt, rs, win)), o...  44.5 us

profile of v8, /device:TPU:1, one launch (start us, length us, event | category | flops | bytes accessed | tf_op | source)
XLA Modules:
  0.0 45.9 jit_solution(11884274899334691290)
XLA Ops:
  0.6 44.5 %shard_map.112 = (bf16[4,2048]{1,0:T(4,128)(2,1)S(1)}, bf16[12,2048]{1,0:T(8,128)(2,1)S(1)}, bf16[128,128]{1,0:T(8,128)(2,1)S(1)}) custom-call(bf16[128,2048]{1,0:T(8,128)(2,1)} %tgt_h.1, bf16[384,2048]{1,0:T(8,128)(2,1)} %src_h.1, bf16[128,2048]{1,0:T(8,128)(2,1)} %cot_h.1, f32[1,2048]{1,0:T(1,128)} %bitcast.2, f32[1,2048]{1,0:T(1,128)} %bitcast.3, ...), custom_call_target="tpu_custom_call" | custom-call | tf_op jit(solution)/shard_map/pallas_call | solution.py:427
  45.2 0.7 %shard_map.113 = (bf16[4,2048]{1,0:T(4,128)(2,1)}, bf16[12,2048]{1,0:T(8,128)(2,1)}, bf16[128,128]{1,0:T(8,128)(2,1)}) custom-call(bf16[4,2048]{1,0:T(4,128)(2,1)S(1)} %get-tuple-element.6.a, bf16[12,2048]{1,0:T(8,128)(2,1)S(1)} %get-tuple-element.7.b, bf16[128,128]{1,0:T(8,128)(2,1)S(1)} %get-tuple-element.8.c), custom_call_target="tpu_custom_call" | custom-call | tf_op jit(solution)/shard_map/pallas_call | solution.py:442
